TPU v7x, 32 devices: a whole 2x2x4 slice. The times are simulated.
32 devices in a mesh: sp: 16 (over z, y, x), dp: 2 (over core).
Axes of the slice: x: 2, y: 2, z: 4, core: 2. Of those that a mesh axis runs over, the one named last changes fastest.
Arguments:
- tokens: bfloat16 [4, 1024, 3072], P('dp', 'sp'), may hold values from -6 to 6
- pre_gain: float32 [3072], replicated, may hold values from 0.1 to 1.9
- in_weight: bfloat16 [3072, 1536], P('dp', 'sp'), may hold values from -0.109375 to 0.109375
- decay_rate: float32 [2, 96, 64], replicated, may hold values from 0 to 1, as said below
- frequency: float32 [2, 96, 64], replicated, may hold values from 1 to 200
- log_step: float32 [2, 96], replicated, may hold values from -3 to -2.3
- input_matrix: float32 [2, 2, 96, 1024], replicated, may hold values from -1 to 1
- output_matrix: float32 [2, 2, 96, 1024], replicated, may hold values from -0.5 to 0.5
- skip_gain: float32 [1536], replicated, may hold values from -4 to 4
- glu_weight: bfloat16 [1536, 1536], P('dp', 'sp'), may hold values from -0.15625 to 0.15625
- up_weight: bfloat16 [1536, 3072], P('dp', 'sp'), may hold values from -0.15625 to 0.15625
- post_gain: float32 [3072], replicated, may hold values from 0.1 to 1.9
Outputs:
- output: bfloat16 [4, 1024, 3072], P('dp', 'sp')
Inputs may be any that keep to these rules, and one draw needn't show every extreme that they name: `decay_rate`: positive, for every direction, group and state.
All inputs are finite; a program needn't handle non-finite values.
Results may differ from a plain program's by a relative error of at most 0.0073.
Values may be sent and summed in bfloat16 or wider, within the bound.
A program may use at most 128 MiB of HBM per device.

v0:
```python
import jax
import jax.numpy as jnp
from jax import lax
from jax.sharding import PartitionSpec as P

highest = lax.Precision.HIGHEST
epsilon = 1e-06


def rms_scale(values, gain):
    widened = values.astype(jnp.float32)
    return widened * lax.rsqrt(jnp.mean(widened * widened, axis=-1, keepdims=True) + epsilon) * gain


def discretize(decay_rate, frequency, log_step, input_matrix):
    groups, states = decay_rate.shape
    delta = jnp.exp(log_step)[:, None]
    damping = -decay_rate * delta
    turning = frequency * delta
    modulus = jnp.exp(damping)
    bar_im = modulus * jnp.sin(turning)
    half_sine = jnp.sin(0.5 * turning)
    minus_re = jnp.expm1(damping) * jnp.cos(turning) - 2.0 * half_sine * half_sine
    denominator = decay_rate * decay_rate + frequency * frequency
    factor_re = (bar_im * frequency - minus_re * decay_rate) / denominator
    factor_im = (-bar_im * decay_rate - minus_re * frequency) / denominator
    matrix_re = input_matrix[0].reshape(groups, states, -1)
    matrix_im = input_matrix[1].reshape(groups, states, -1)
    bbar_re = factor_re[..., None] * matrix_re - factor_im[..., None] * matrix_im
    bbar_im = factor_re[..., None] * matrix_im + factor_im[..., None] * matrix_re
    return (damping, turning, bbar_re, bbar_im)


def block_direction(blocks, damping, turning, bbar_re, bbar_im, out_re, out_im, reverse):
    leading = blocks.shape[1:3]
    block_len = blocks.shape[-1]
    zero_state = jnp.zeros(leading + (damping.shape[1],), jnp.float32)
    boundary = 0 if reverse else -1
    position = jnp.arange(block_len, dtype=jnp.float32)
    exponent = block_len - 1.0 - position if reverse else position
    angle = turning[..., None] * exponent
    cosine = jnp.cos(angle)
    sine = jnp.sin(angle)
    grow = jnp.exp(damping[..., None] * exponent)
    shrink = jnp.exp(-damping[..., None] * exponent)
    power_re = grow * cosine
    power_im = grow * sine
    inverse_re = shrink * cosine
    inverse_im = -shrink * sine
    next_angle = turning[..., None] * (exponent + 1.0)
    next_grow = jnp.exp(damping[..., None] * (exponent + 1.0))
    carry_re = next_grow * jnp.cos(next_angle)
    carry_im = next_grow * jnp.sin(next_angle)
    rows = jnp.arange(block_len)[:, None]
    columns = jnp.arange(block_len)[None, :]
    triangle = jnp.where(rows >= columns if reverse else rows <= columns, 1.0, 0.0).astype(
        jnp.float32
    )

    def advance(carried, block):
        drive_re = jnp.einsum("kph,skhq->skpq", bbar_re, block, precision=highest)
        drive_im = jnp.einsum("kph,skhq->skpq", bbar_im, block, precision=highest)
        scaled_re = drive_re * inverse_re - drive_im * inverse_im
        scaled_im = drive_re * inverse_im + drive_im * inverse_re
        total_re = jnp.einsum("skpj,jq->skpq", scaled_re, triangle, precision=highest)
        total_im = jnp.einsum("skpj,jq->skpq", scaled_im, triangle, precision=highest)
        held_re = carried[0][..., None]
        held_im = carried[1][..., None]
        state_re = (
            power_re * total_re - power_im * total_im + carry_re * held_re - carry_im * held_im
        )
        state_im = (
            power_re * total_im + power_im * total_re + carry_re * held_im + carry_im * held_re
        )
        passed = (state_re[..., boundary], state_im[..., boundary])
        result = jnp.einsum("khp,skpq->skhq", out_re, state_re, precision=highest) - jnp.einsum(
            "khp,skpq->skhq", out_im, state_im, precision=highest
        )
        return (passed, result)

    unused, outputs = lax.scan(advance, (zero_state, zero_state), blocks, reverse=reverse)
    return outputs


def per_device(
    tokens,
    pre_gain,
    in_weight,
    decay_rate,
    frequency,
    log_step,
    input_matrix,
    output_matrix,
    skip_gain,
    glu_weight,
    up_weight,
    post_gain,
):
    normed = rms_scale(tokens, pre_gain).astype(jnp.bfloat16)
    in_cols, glu_cols, up_cols = (
        lax.all_gather(in_weight, "dp", axis=0, tiled=True),
        lax.all_gather(glu_weight, "dp", axis=0, tiled=True),
        lax.all_gather(up_weight, "dp", axis=0, tiled=True),
    )
    mixer_in = jnp.einsum(
        "std,dw->swt",
        normed,
        lax.all_gather(in_cols, "sp", axis=1, tiled=True),
        preferred_element_type=jnp.float32,
    ).astype(jnp.bfloat16)
    glu_full, up_full = (
        lax.all_gather(glu_cols, "sp", axis=1, tiled=True),
        lax.all_gather(up_cols, "sp", axis=1, tiled=True),
    )
    gathered = lax.all_to_all(mixer_in, "sp", split_axis=1, concat_axis=2, tiled=True)
    seq_count, width_dev, length = gathered.shape
    group_size = input_matrix.shape[-1] // decay_rate.shape[2]
    own_groups = width_dev // group_size
    offset = lax.axis_index("sp") * own_groups
    block_len = min(128, length)
    block_count = length // block_len
    widened = gathered.astype(jnp.float32)
    blocks = jnp.moveaxis(
        widened.reshape(seq_count, own_groups, group_size, block_count, block_len), 3, 0
    )
    summed = None
    for direction in range(2):
        rates = lax.dynamic_slice_in_dim(decay_rate[direction], offset, own_groups, 0)
        frequencies = lax.dynamic_slice_in_dim(frequency[direction], offset, own_groups, 0)
        log_steps = lax.dynamic_slice_in_dim(log_step[direction], offset, own_groups, 0)
        matrix = lax.dynamic_slice_in_dim(input_matrix[direction], offset, own_groups, 1)
        readout = lax.dynamic_slice_in_dim(output_matrix[direction], offset, own_groups, 1)
        damping, turning, bbar_re, bbar_im = discretize(rates, frequencies, log_steps, matrix)
        out_re = readout[0].reshape(own_groups, group_size, -1)
        out_im = readout[1].reshape(own_groups, group_size, -1)
        partial_value = block_direction(
            blocks, damping, turning, bbar_re, bbar_im, out_re, out_im, direction == 1
        )
        summed = partial_value if summed is None else summed + partial_value
    scanned = jnp.moveaxis(summed, 0, 3).reshape(seq_count, width_dev, length)
    skip_rows = lax.dynamic_slice_in_dim(skip_gain, offset * group_size, width_dev, 0)
    mixed_rows = jax.nn.gelu(scanned + skip_rows[None, :, None] * widened).astype(jnp.bfloat16)
    mixed_rows = lax.all_to_all(mixed_rows, "sp", split_axis=2, concat_axis=1, tiled=True)
    gate_pre = jnp.einsum("swt,wv->svt", mixed_rows, glu_full, preferred_element_type=jnp.float32)
    gated_rows = (mixed_rows.astype(jnp.float32) * jax.nn.sigmoid(gate_pre)).astype(jnp.bfloat16)
    projected = jnp.einsum("swt,wd->std", gated_rows, up_full, preferred_element_type=jnp.float32)
    return rms_scale(projected, post_gain).astype(jnp.bfloat16)


def solution(mesh):
    return jax.shard_map(
        per_device,
        mesh=mesh,
        in_specs=(
            P("dp", "sp", None),
            P(),
            P("dp", "sp"),
            P(),
            P(),
            P(),
            P(),
            P(),
            P(),
            P("dp", "sp"),
            P("dp", "sp"),
            P(),
        ),
        out_specs=P("dp", "sp", None),
        check_vma=False,
    )
```

profile of v0, /device:TPU:0, one launch (start us, length us, event | category | flops | bytes accessed | tf_op | source)
XLA Modules:
  0.0 370.2 jit_solution(14923406609285104885)
XLA Ops:
  6.5 4.4 %all_gather.18 = bf16[3072,96]{0,1:T(8,128)(2,1)} all-gather(bf16[1536,96]{0,1:T(8,128)(2,1)} %param.18), channel_id=1, replica_groups=mesh['sp'=16,'dp'=2] {'dp'}, dimensions={0}, use_global_device_ids=true | all-gather | bytes 884736 | tf_op jit(solution)/shard_map/all_gather | solution.py:101
  11.0 2.3 all_gather.20
  13.4 2.4 all_gather.22
  17.3 1.3 fusion.175
  18.6 1.6 constant_dynamic-slice_fusion
  20.6 1.0 copy-done
  22.8 112.4 %all-gather.4.cloned.1.call-done = bf16[3072,1536]{0,1:T(8,128)(2,1)} async-done(((bf16[3072,96]{0,1:T(8,128)(2,1)}), bf16[3072,1536]{0,1:T(8,128)(2,1)}) %all-gather.4.cloned.1.call-update) | async-done | bytes 9437200 | tf_op jit(solution)/shard_map/all_gather | solution.py:108
  135.2 6.9 %fusion.121 = bf16[2,1536,64]{1,2,0:T(8,128)(2,1)S(1)} fusion(bf16[3072,1536]{0,1:T(8,128)(2,1)} %all-gather.4.cloned.1.call-done, bf16[2,64,3072]{2,1,0:T(8,128)(2,1)S(1)} %copy-done, f32[3072]{0:T(1024)S(1)} %copy-done.19, f32[2,64]{1,0:T(2,128)S(1)} %add_rsqrt_fusion.1), kind=kOutput, calls=%fused_computation.129 | convolution fusion | flops 1209729024 | bytes 10629632 | tf_op jit(solution)/shard_map/std,dw->swt/dot_general | solution.py:105
  142.8 1.3 reshape.458
  144.1 3.8 %all-to-all-start = ((bf16[16,2,6144]{2,1,0:T(2,128)(2,1)}), bf16[16,2,6144]{2,1,0:T(2,128)(2,1)S(1)}, u32[]{:S(2)}, u32[]{:S(2)}) async-start(bf16[16,2,6144]{2,1,0:T(2,128)(2,1)} %reshape.458), calls=%async_computation | async-start | bytes 786432 | tf_op jit(solution)/shard_map/all_to_all | solution.py:115
  152.5 1.4 dynamic_slice.68
  154.4 10.1 %all-to-all-done = bf16[16,2,6144]{2,1,0:T(2,128)(2,1)S(1)} async-done(((bf16[16,2,6144]{2,1,0:T(2,128)(2,1)}), bf16[16,2,6144]{2,1,0:T(2,128)(2,1)S(1)}, u32[]{:S(2)}, u32[]{:S(2)}) %all-to-all-start) | async-done | bytes 393248 | tf_op jit(solution)/shard_map/all_to_all | solution.py:115
  167.0 54.4 %while.38 = (s32[]{:T(128)}, f32[2,6,64]{2,0,1:T(2,128)S(1)}, f32[2,6,64]{2,0,1:T(2,128)S(1)}, f32[8,2,6,16,128]{4,3,1,2,0:T(8,128)}, f32[8,2,6,16,128]{4,3,1,2,...) while((s32[]{:T(128)}, f32[2,6,64]{2,0,1:T(2,128)S(1)}, ...), condition=%wide.region_2.3_spmd.clone.clone.clone, body=%wide.region_1.2_spmd.clone.clone.clone.sunk | while | flops 380133376 | bytes 7960425 | solution.py:81
  167.0 1.5 fusion.214
  168.6 1.3 convolution_bitcast_fusion.6
  172.1 1.0 fusion.217
  173.8 1.5 fusion.214
  175.4 1.3 convolution_bitcast_fusion.6
  178.9 1.0 fusion.217
  180.6 1.5 fusion.214
  182.2 1.3 convolution_bitcast_fusion.6
  185.7 1.0 fusion.217
  187.4 1.5 fusion.214
  189.0 1.4 convolution_bitcast_fusion.6
  192.5 1.0 fusion.217
  194.2 1.5 fusion.214
  195.8 1.3 convolution_bitcast_fusion.6
  199.3 1.0 fusion.217
  201.0 1.5 fusion.214
  202.6 1.3 convolution_bitcast_fusion.6
  206.1 1.0 fusion.217
  207.8 1.5 fusion.214
  209.4 1.3 convolution_bitcast_fusion.6
  212.9 1.0 fusion.217
  214.6 1.5 fusion.214
  216.2 1.3 convolution_bitcast_fusion.6
  219.7 1.0 fusion.217
  221.4 1.2 copy.105
  222.7 1.0 broadcast.255.clone.1
  224.3 66.4 %while.39 = (s32[]{:T(128)}, f32[2,6,64]{2,0,1:T(2,128)}, f32[2,6,64]{2,0,1:T(2,128)S(1)}, f32[8,2,6,16,128]{4,3,1,2,0:T(8,128)}, f32[8,2,6,16,128]{4,3,1,2,0:T(...) while((s32[]{:T(128)}, f32[2,6,64]{2,0,1:T(2,128)}, ...), condition=%wide.region_4.5_spmd.clone.clone.clone, body=%wide.region_3.4_spmd.clone.clone.clone.sunk | while | flops 380133376 | bytes 7728813 | solution.py:81
  224.3 2.2 fusion.226
  226.5 1.3 convolution_bitcast_fusion.7
  232.5 2.3 fusion.226
  234.8 1.3 convolution_bitcast_fusion.7
  238.9 1.0 fusion.229
  240.8 2.3 fusion.226
  243.0 1.3 convolution_bitcast_fusion.7
  249.1 2.2 fusion.226
  251.3 1.4 convolution_bitcast_fusion.7
  255.5 1.0 fusion.229
  257.4 2.3 fusion.226
  259.6 1.3 convolution_bitcast_fusion.7
  265.6 2.3 fusion.226
  267.9 1.3 convolution_bitcast_fusion.7
  272.0 1.0 fusion.229
  273.9 2.3 fusion.226
  276.2 1.3 convolution_bitcast_fusion.7
  282.2 2.2 fusion.226
  284.4 1.3 convolution_bitcast_fusion.7
  290.7 1.5 add_bitcast_fusion
  294.1 26.7 %all_to_all.27 = bf16[2,96,1024]{1,0,2:T(2,128)(2,1)S(1)} all-to-all(bf16[2,96,1024]{1,0,2:T(2,128)(2,1)S(1)} %copy.119), channel_id=1, replica_groups=mesh['sp'=16,'dp'=2] {'sp'}, dimensions={2} | all-to-all | bytes 786432 | tf_op jit(solution)/shard_map/all_to_all | solution.py:143
  321.8 30.8 %all-gather.8.cloned.1.call-done = bf16[1536,3072]{0,1:T(8,128)(2,1)} async-done(((bf16[1536,192]{0,1:T(8,128)(2,1)}), bf16[1536,3072]{0,1:T(8,128)(2,1)}) %all-gather.8.cloned.1.call-update) | async-done | bytes 9437200 | tf_op jit(solution)/shard_map/all_gather | solution.py:113
  352.6 9.9 %multiply_reduce_fusion = (f32[2,64]{1,0:T(2,128)S(1)}, f32[2,64,3072]{2,1,0:T(8,128)S(1)}) fusion(bf16[1536,3072]{0,1:T(8,128)(2,1)} %all-gather.8.cloned.1.call-done, bf16[2,1536,64]{1,2,0:T(8,128)(2,1)S(1)} %all_to_all.24, bf16[1536,1536]{0,1:T(8,128)(2,1)} %all-gather.6.cloned.1.call-done), kind=kOutput, calls=%fused_computation.141 | convolution fusion | flops 1813905280 | bytes 16122368 | tf_op jit(solution)/shard_map/swt,wd->std/dot_general | solution.py:146
  362.5 1.1 multiply_convert_fusion
  (354 shorter events, 70.9 us)
Async XLA Ops:
  6.5 4.4 %copy-start.12 = (bf16[768,96]{0,1:T(8,128)(2,1)S(1)}, bf16[768,96]{0,1:T(8,128)(2,1)}, u32[]{:S(2)}) copy-start(bf16[768,96]{0,1:T(8,128)(2,1)} %param.25) | copy-start | bytes 442372
  6.5 6.8 %copy-start.5 = (bf16[768,192]{0,1:T(8,128)(2,1)S(1)}, bf16[768,192]{0,1:T(8,128)(2,1)}, u32[]{:S(2)}) copy-start(bf16[768,192]{0,1:T(8,128)(2,1)} %param.26) | copy-start | bytes 884740
  6.5 128.7 %all-gather.4.cloned.1.call-start = ((), (), s32[]{:S(2)}) async-start(), calls=%async_computation.2 | async-start | bytes 10027008 | tf_op jit(solution)/shard_map/all_gather | solution.py:108
  10.9 4.9 %copy-start.17 = (f32[2,96,64]{1,2,0:T(8,128)S(1)}, f32[2,96,64]{1,2,0:T(8,128)}, u32[]{:S(2)}) copy-start(f32[2,96,64]{1,2,0:T(8,128)} %param.19) | copy-start | bytes 147460
  10.9 5.5 %copy-start.18 = (f32[2,96,64]{1,2,0:T(8,128)S(1)}, f32[2,96,64]{1,2,0:T(8,128)}, u32[]{:S(2)}) copy-start(f32[2,96,64]{1,2,0:T(8,128)} %param.20) | copy-start | bytes 147460
  10.9 6.3 %copy-start.23 = (f32[2,96]{1,0:T(2,128)S(1)}, f32[2,96]{1,0:T(2,128)}, u32[]{:S(2)}) copy-start(f32[2,96]{1,0:T(2,128)} %param.21) | copy-start | bytes 2308
  10.9 6.4 %copy-start.3 = (f32[2,2,96,1024]{3,2,1,0:T(8,128)S(1)}, f32[2,2,96,1024]{3,2,1,0:T(8,128)}, u32[]{:S(2)}) copy-start(f32[2,2,96,1024]{3,2,1,0:T(8,128)} %param.22) | copy-start | bytes 4718596
  10.9 310.9 %all-gather.6.cloned.1.call-start = ((), (), s32[]{:S(2)}) async-start(), calls=%async_computation.3 | async-start | bytes 5013504 | tf_op jit(solution)/shard_map/all_gather | solution.py:112
  13.3 339.3 %all-gather.8.cloned.1.call-start = ((), (), s32[]{:S(2)}) async-start(), calls=%async_computation.4 | async-start | bytes 10027008 | tf_op jit(solution)/shard_map/all_gather | solution.py:113
  17.3 3.1 copy-start.4
  20.4 1.2 copy-start
  21.6 113.7 %copy-start.19 = (f32[3072]{0:T(1024)S(1)}, f32[3072]{0:T(1024)}, u32[]{:S(2)}) copy-start(f32[3072]{0:T(1024)} %param.17) | copy-start | bytes 36868
  142.2 5.7 %copy-start.13 = (f32[1,96,64]{1,2,0:T(8,128)S(1)}, f32[1,96,64]{1,2,0:T(8,128)}, u32[]{:S(2)}) copy-start(f32[1,96,64]{1,2,0:T(8,128)} %get-tuple-element.879) | copy-start | bytes 73732
  142.2 5.7 %copy-start.14 = (f32[1,96,64]{1,2,0:T(8,128)S(1)}, f32[1,96,64]{1,2,0:T(8,128)}, u32[]{:S(2)}) copy-start(f32[1,96,64]{1,2,0:T(8,128)} %get-tuple-element.881) | copy-start | bytes 73732
  142.8 6.4 %copy-start.16 = (f32[1,1,6,1024]{3,2,1,0:T(8,128)S(1)}, f32[1,1,6,1024]{3,2,1,0:T(8,128)}, u32[]{:S(2)}) copy-start(f32[1,1,6,1024]{3,2,1,0:T(8,128)} %get-tuple-element.897) | copy-start | bytes 73732
  142.8 6.5 %copy-start.15 = (f32[1,1,6,1024]{3,2,1,0:T(8,128)S(1)}, f32[1,1,6,1024]{3,2,1,0:T(8,128)}, u32[]{:S(2)}) copy-start(f32[1,1,6,1024]{3,2,1,0:T(8,128)} %get-tuple-element.896) | copy-start | bytes 73732
  144.1 20.5 %all-to-all-start = ((bf16[16,2,6144]{2,1,0:T(2,128)(2,1)}), bf16[16,2,6144]{2,1,0:T(2,128)(2,1)S(1)}, u32[]{:S(2)}, u32[]{:S(2)}) async-start(bf16[16,2,6144]{2,1,0:T(2,128)(2,1)} %reshape.458), calls=%async_computation | async-start | bytes 786432 | tf_op jit(solution)/shard_map/all_to_all | solution.py:115
  165.8 1.2 copy-start.6
  165.8 1.2 copy-start.8
  165.8 1.2 copy-start.10
  167.0 3.5 copy-start.20
  172.0 1.7 copy-start.7
  172.0 1.7 copy-start.9
  172.1 1.7 copy-start.11
  172.1 1.7 copy-start.21
  173.8 3.5 copy-start.20
  177.3 1.1 copy-start.1
  178.8 1.7 copy-start.7
  178.9 1.7 copy-start.9
  178.9 1.7 copy-start.11
  178.9 1.7 copy-start.21
  180.6 3.5 copy-start.20
  185.6 1.7 copy-start.7
  185.6 1.7 copy-start.9
  185.7 1.7 copy-start.11
  185.7 1.7 copy-start.21
  187.4 3.5 copy-start.20
  191.0 1.1 copy-start.1
  192.4 1.7 copy-start.7
  192.5 1.7 copy-start.9
  192.5 1.7 copy-start.11
  192.5 1.7 copy-start.21
  194.2 3.5 copy-start.20
  197.8 1.1 copy-start.1
  199.3 1.7 copy-start.7
  199.3 1.7 copy-start.9
  199.3 1.7 copy-start.11
  199.3 1.7 copy-start.21
  201.0 3.5 copy-start.20
  206.0 1.7 copy-start.7
  206.1 1.7 copy-start.9
  206.1 1.7 copy-start.11
  206.1 1.7 copy-start.21
  207.8 3.5 copy-start.20
  212.8 1.7 copy-start.7
  212.9 1.7 copy-start.9
  212.9 1.7 copy-start.11
  212.9 1.7 copy-start.21
  214.6 3.5 copy-start.20
  219.7 1.7 copy-start.7
  219.7 1.7 copy-start.9
  219.7 1.7 copy-start.11
  219.7 1.7 copy-start.21
  321.8 40.8 %copy-start.22 = (f32[3072]{0:T(1024)S(1)}, f32[3072]{0:T(1024)}, u32[]{:S(2)}) copy-start(f32[3072]{0:T(1024)} %param.27) | copy-start | bytes 36868
  (14 other events, 14.8 us)
Sparse Core Ops, SparseCore 0:
  11.1 124.1 all-gather.3
  138.0 82.1 all-gather.5
  223.0 129.6 all-gather.7
where the time goes:
time: 372 us; the launch traced here: 370 us
  waiting for transfers between devices  153 us (41%)
  matrix products  86.5 us (23%)
  local copies, waits for them, and re-layouts  39.2 us (11%)
  other arithmetic  35.8 us (10%)
  blocking collectives  35.7 us (10%)
  between operations  13.5 us (4%)
  starting transfers between devices  3.89 us (1%)
    all_gather x1, waiting for transfers between devices, per_device(): lax.all_gather(in_cols, 'sp', axis=1, tiled=True)  112 us
    all_gather x1, waiting for transfers between devices, per_device(): lax.all_gather(up_cols, 'sp', axis=1, tiled=True)  30.8 us
    all_to_all x1, blocking collectives, per_device(): lax.all_to_all(mixed_rows, 'sp', split_axis=2, concat_axis=1, tiled=True)  26.7 us
    dot_general x16, matrix products, advance(): drive_re = jnp.einsum('kph,skhq->skpq', bbar_re, block, precision=highest)  21.4 us
    mul x8, other arithmetic, block_direction(): power_re = grow * cosine  18 us
    dot_general x16, matrix products, advance(): jnp.einsum('khp,skpq->skhq', out_im, state_im, precision=highest)  15.7 us
    slice x48, local copies, waits for them, and re-layouts, advance(): passed = (state_re[..., boundary], state_im[..., boundary])  12.8 us
    mul x8, other arithmetic, block_direction(): carry_re = next_grow * jnp.cos(next_angle)  12.3 us
  transfers between devices with their start and end apart: 4, of which 3 were waited for; matrix products, arithmetic and copies ran while one was open for 40% of the time, Pallas kernels for 0%

commit v1 on v0

v1 whole, which is shorter than its diff:
```python
import functools

import jax
import jax.numpy as jnp
from jax import lax
from jax.experimental import pallas as pl
from jax.experimental.pallas import tpu as pltpu
from jax.sharding import PartitionSpec as P

epsilon = 1e-06
BLOCK = 16


def rms_scale(values, gain):
    widened = values.astype(jnp.float32)
    return widened * lax.rsqrt(jnp.mean(widened * widened, axis=-1, keepdims=True) + epsilon) * gain


def own_tables(decay_rate, frequency, log_step, input_matrix, output_matrix, offset, own, hop_steps):
    take = functools.partial(lax.dynamic_slice_in_dim, start_index=offset, slice_size=own)
    rates = take(decay_rate, axis=1)
    frequencies = take(frequency, axis=1)
    delta = jnp.exp(take(log_step, axis=1))[..., None]
    damping = -rates * delta
    turning = frequencies * delta
    modulus = jnp.exp(damping)
    bar_im = modulus * jnp.sin(turning)
    half_sine = jnp.sin(0.5 * turning)
    minus_re = jnp.expm1(damping) * jnp.cos(turning) - 2.0 * half_sine * half_sine
    denominator = rates * rates + frequencies * frequencies
    factor_re = (bar_im * frequencies - minus_re * rates) / denominator
    factor_im = (-bar_im * rates - minus_re * frequencies) / denominator
    states = rates.shape[-1]
    matrix = take(input_matrix, axis=2).reshape(2, 2, own, states, -1)
    readout = take(output_matrix, axis=2).reshape(2, 2, own, -1, states)
    bbar_re = factor_re[..., None] * matrix[:, 0] - factor_im[..., None] * matrix[:, 1]
    bbar_im = factor_re[..., None] * matrix[:, 1] + factor_im[..., None] * matrix[:, 0]

    def lanes(value):
        return jnp.transpose(value, (1, 2, 0, 3)).reshape(own, value.shape[2], 2 * states)

    b_re = lanes(jnp.swapaxes(bbar_re, 2, 3))
    b_im = lanes(jnp.swapaxes(bbar_im, 2, 3))
    c_re = lanes(readout[:, 0])
    c_im = lanes(readout[:, 1])
    step = jnp.arange(BLOCK, dtype=jnp.float32)
    last = BLOCK - 1.0
    hops = BLOCK * 2.0 ** jnp.arange(hop_steps, dtype=jnp.float32)
    forward = jnp.concatenate([last - step, step + 1.0, step - last, hops])
    backward = jnp.concatenate([step, BLOCK - step, -step, hops])
    exponent = jnp.stack([forward, backward])[:, None, :, None]
    size = jnp.exp(damping[:, :, None, :] * exponent)
    angle = turning[:, :, None, :] * exponent
    return b_re, b_im, c_re, c_im, lanes(size * jnp.cos(angle)), lanes(size * jnp.sin(angle))


def table_kernel(b_re, b_im, c_re, c_im, p_re, p_im, within, enter, leave, inner_ref):
    channels, lanes = b_re.shape[1:]
    bre, bim, cre, cim = b_re[0], b_im[0], c_re[0], c_im[0]
    for step in range(BLOCK):
        rows = pl.ds(step * channels, channels)

        def power(which):
            row = which * BLOCK + step
            return p_re[0, row : row + 1, :], p_im[0, row : row + 1, :]

        wre, wim = power(0)
        enter[0, rows, :lanes] = (wre * bre - wim * bim).astype(jnp.bfloat16)
        enter[0, rows, lanes:] = (wre * bim + wim * bre).astype(jnp.bfloat16)
        vre, vim = power(1)
        leave[0, rows, :lanes] = (vre * cre - vim * cim).astype(jnp.bfloat16)
        leave[0, rows, lanes:] = (-vre * cim - vim * cre).astype(jnp.bfloat16)
        xre, xim = power(2)
        inner_ref[rows, :lanes] = (xre * cre - xim * cim).astype(jnp.bfloat16)
        inner_ref[rows, lanes:] = (-xre * cim - xim * cre).astype(jnp.bfloat16)
    side = enter[0].shape[0]
    lane = lax.broadcasted_iota(jnp.int32, (side, 2 * lanes), 1) % lanes
    entering = enter[0]
    contract = (((1,), (1,)), ((), ()))
    zero = jnp.zeros_like(entering)
    ahead = lax.dot_general(
        jnp.where(lane < lanes // 2, entering, zero), inner_ref[...], contract,
        preferred_element_type=jnp.float32,
    )
    behind = lax.dot_general(
        jnp.where(lane < lanes // 2, zero, entering), inner_ref[...], contract,
        preferred_element_type=jnp.float32,
    )
    source = lax.broadcasted_iota(jnp.int32, (side, side), 0) // channels
    target = lax.broadcasted_iota(jnp.int32, (side, side), 1) // channels
    within[0] = (
        jnp.where(source <= target, ahead, 0.0) + jnp.where(source >= target, behind, 0.0)
    ).astype(jnp.bfloat16)


def make_tables(tables):
    own, channels, lanes = tables[0].shape
    side = BLOCK * channels
    whole = lambda value: pl.BlockSpec((1,) + value.shape[1:], lambda g: (g, 0, 0))
    out = lambda width: jax.ShapeDtypeStruct((own, side, width), jnp.bfloat16)
    outs = (out(side), out(2 * lanes), out(2 * lanes))
    return pl.pallas_call(
        table_kernel,
        grid=(own,),
        out_shape=outs,
        in_specs=[whole(value) for value in tables],
        out_specs=[whole(value) for value in outs],
        scratch_shapes=[pltpu.VMEM((side, 2 * lanes), jnp.bfloat16)],
        cost_estimate=pl.CostEstimate(
            flops=own * 4 * side * side * 2 * lanes * 4, bytes_accessed=own * side * side * 6, transcendentals=0
        ),
        name="tables",
    )(*tables)


def scan_kernel(length, u_ref, within, enter, leave, p_re, p_im, skip, out_ref):
    lanes = p_re.shape[2]
    rows = u_ref.shape[1]
    u = u_ref[0]
    local = jnp.dot(u, enter[0], preferred_element_type=jnp.float32)
    s_re, s_im = local[:, :lanes], local[:, lanes:]
    lane = lax.broadcasted_iota(jnp.int32, (rows, lanes), 1)
    place = lax.broadcasted_iota(jnp.int32, (rows, lanes), 0) % length
    forward = lane < lanes // 2

    def shifted(value, by):
        pad = jnp.zeros((by, lanes), jnp.float32)
        down = jnp.concatenate([pad, value[:-by]], axis=0)
        up = jnp.concatenate([value[by:], pad], axis=0)
        down = jnp.where(place >= by, down, 0.0)
        up = jnp.where(place < length - by, up, 0.0)
        return jnp.where(forward, down, up)

    hop = 1
    row = 3 * BLOCK
    while hop < length:
        h_re, h_im = p_re[0, row : row + 1, :], p_im[0, row : row + 1, :]
        m_re, m_im = shifted(s_re, hop), shifted(s_im, hop)
        s_re, s_im = s_re + h_re * m_re - h_im * m_im, s_im + h_re * m_im + h_im * m_re
        hop, row = 2 * hop, row + 1
    held = jnp.concatenate([shifted(s_re, 1), shifted(s_im, 1)], axis=1).astype(jnp.bfloat16)
    total = jnp.dot(u, within[0], preferred_element_type=jnp.float32)
    total += lax.dot_general(
        held, leave[0], (((1,), (1,)), ((), ())), preferred_element_type=jnp.float32
    )
    out_ref[0] = jax.nn.gelu(total + skip[0] * u.astype(jnp.float32)).astype(jnp.bfloat16)


def run_scan(blocks, within, enter, leave, p_re, p_im, skip, length):
    own, rows, side = blocks.shape
    whole = lambda value: pl.BlockSpec((1,) + value.shape[1:], lambda g: (g, 0, 0))
    operands = (blocks, within, enter, leave, p_re, p_im, skip)
    return pl.pallas_call(
        functools.partial(scan_kernel, length),
        grid=(own,),
        out_shape=jax.ShapeDtypeStruct(blocks.shape, jnp.bfloat16),
        in_specs=[whole(value) for value in operands],
        out_specs=whole(blocks),
        name="mixer",
    )(*operands)


def per_device(
    tokens,
    pre_gain,
    in_weight,
    decay_rate,
    frequency,
    log_step,
    input_matrix,
    output_matrix,
    skip_gain,
    glu_weight,
    up_weight,
    post_gain,
):
    def gather(weight):
        columns = lax.all_gather(weight, "sp", axis=1, tiled=True)
        return lax.all_gather(columns, "dp", axis=0, tiled=True)

    seqs, local_len, _ = tokens.shape
    sp = lax.axis_size("sp")
    group_size = input_matrix.shape[-1] // decay_rate.shape[2]
    groups = decay_rate.shape[1]
    own = groups // sp
    near = local_len // BLOCK
    side = BLOCK * group_size
    length = near * sp
    offset = lax.axis_index("sp") * own

    in_full = gather(in_weight)
    tables = own_tables(
        decay_rate, frequency, log_step, input_matrix, output_matrix, offset, own,
        max(1, (length - 1).bit_length()),
    )
    within, enter, leave = make_tables(tables)
    skip_rows = lax.dynamic_slice_in_dim(skip_gain.reshape(groups, 1, group_size), offset, own, 0)
    skip_rows = jnp.tile(skip_rows, (1, 1, BLOCK))
    normed = rms_scale(tokens, pre_gain).astype(jnp.bfloat16)
    mixer_in = jnp.einsum(
        "std,dw->stw", normed, in_full, preferred_element_type=jnp.float32
    ).astype(jnp.bfloat16)
    glu_full, up_full = gather(glu_weight), gather(up_weight)
    blocks = mixer_in.reshape(seqs, near, BLOCK, groups, group_size)
    blocks = jnp.transpose(blocks, (3, 0, 1, 2, 4)).reshape(groups, seqs, near, side)
    blocks = lax.all_to_all(blocks, "sp", split_axis=0, concat_axis=2, tiled=True)
    mixed = run_scan(
        blocks.reshape(own, seqs * length, side), within, enter, leave, tables[4], tables[5],
        skip_rows, length,
    )
    mixed = mixed.reshape(own, seqs, length, side)
    mixed = lax.all_to_all(mixed, "sp", split_axis=2, concat_axis=0, tiled=True)
    mixed = mixed.reshape(groups, seqs, near, BLOCK, group_size)
    mixed = jnp.transpose(mixed, (1, 2, 3, 0, 4)).reshape(seqs, local_len, groups * group_size)
    gate_pre = jnp.einsum("stw,wv->stv", mixed, glu_full, preferred_element_type=jnp.float32)
    gated = (mixed.astype(jnp.float32) * jax.nn.sigmoid(gate_pre)).astype(jnp.bfloat16)
    projected = jnp.einsum("stw,wd->std", gated, up_full, preferred_element_type=jnp.float32)
    return rms_scale(projected, post_gain).astype(jnp.bfloat16)


def solution(mesh):
    return jax.shard_map(
        per_device,
        mesh=mesh,
        in_specs=(
            P("dp", "sp", None),
            P(),
            P("dp", "sp"),
            P(),
            P(),
            P(),
            P(),
            P(),
            P(),
            P("dp", "sp"),
            P("dp", "sp"),
            P(),
        ),
        out_specs=P("dp", "sp", None),
        check_vma=False,
    )
```

time: 372 us -> 348 us (0.935)
  waiting for transfers between devices: 153 us -> 229 us
  matrix products: 86.5 us -> 12.5 us
  other arithmetic: 35.8 us -> 5.28 us
  blocking collectives: 35.7 us -> 19.2 us
  Pallas kernels: 0 us -> 11.4 us
  local copies, waits for them, and re-layouts: 39.2 us -> 48.8 us
    all_gather x3 -> x6, waiting for transfers between devices: 143 us -> 227 us  [the longest x3 217 us: gather(): columns = lax.all_gather(weight, 'sp', axis=1, tiled=True)]
    dot_general x98 -> x2, matrix products: 86.5 us -> 12.5 us  [the longest x1 7.35 us: per_device(): jnp.einsum('stw,wd->std', gated, up_full, preferred_element_type=jnp.floa...]
    mul x16 -> x3, other arithmetic: 30.3 us -> 1.98 us  [the longest x1 1.36 us: own_tables(): size * jnp.sin(angle)]
    reshape x1 -> x13, local copies, waits for them, and re-layouts: 0.12 us -> 18.7 us  [the longest x1 6.15 us: per_device(): jnp.transpose(mixed, (1, 2, 3, 0, 4))]
    all_gather x0 -> x3, local copies, waits for them, and re-layouts: none -> 17.6 us  [gather(): columns = lax.all_gather(weight, 'sp', axis=1, tiled=True)]
    slice x55 -> x0, local copies, waits for them, and re-layouts: 17.1 us -> none  [the longest x48 12.8 us: advance(): passed = (state_re[..., boundary], state_im[..., boundary])]
    pallas_call x0 -> x2, Pallas kernels: none -> 11.4 us  [the longest x1 6.36 us: run_scan(): pl.pallas_call(functools.partial(scan_kernel, length), grid=(own,), out_s...]
    all_to_all x1, waiting for transfers between devices: 10.1 us -> 0.03 us  [per_device(): lax.all_to_all(blocks, 'sp', split_axis=0, concat_axis=2, tiled=True)]
  transfers between devices with their start and end apart: 4 -> 7, of which waited for: 3 -> 4; matrix products, arithmetic and copies ran while one was open for 40% -> 16% of each run, Pallas kernels for 0% -> 3%
where the time goes in v1:
time: 348 us; the launch traced here: 347 us
  waiting for transfers between devices  229 us (66%)
  local copies, waits for them, and re-layouts  48.8 us (14%)
  blocking collectives  19.2 us (6%)
  between operations  13.7 us (4%)
  matrix products  12.5 us (4%)
  Pallas kernels  11.4 us (3%)
  starting transfers between devices  7 us (2%)
  other arithmetic  5.28 us (2%)
    all_gather x3, waiting for transfers between devices, gather(): columns = lax.all_gather(weight, 'sp', axis=1, tiled=True)  217 us
    all_to_all x1, blocking collectives, per_device(): mixed = lax.all_to_all(mixed, 'sp', split_axis=2, concat_axis=0, tiled=True)  19.2 us
    all_gather x3, local copies, waits for them, and re-layouts, gather(): columns = lax.all_gather(weight, 'sp', axis=1, tiled=True)  17.6 us
    all_gather x3, waiting for transfers between devices, gather(): return lax.all_gather(columns, 'dp', axis=0, tiled=True)  9.47 us
    dot_general x1, matrix products, per_device(): jnp.einsum('stw,wd->std', gated, up_full, preferred_element_type=jnp.floa...  7.35 us
  transfers between devices with their start and end apart: 7, of which 4 were waited for; matrix products, arithmetic and copies ran while one was open for 16% of the time, Pallas kernels for 3%

profile of v1, /device:TPU:0, one launch (start us, length us, event | category | flops | bytes accessed | tf_op | source)
XLA Modules:
  0.0 346.8 jit_solution(14517032142942496132)
XLA Ops:
  6.5 0.7 all-gather.7.cloned.1.call-update
  7.3 0.0 all-gather.11.cloned.1.call-start
  7.3 0.7 all-gather.11.cloned.1.call-update
  8.0 0.0 all-gather.15.cloned.1.call-start
  8.1 0.7 all-gather.15.cloned.1.call-update
  8.7 0.0 all-gather.9.cloned.1.call-start
  8.8 83.8 %all-gather.7.cloned.1.call-done = bf16[1536,1536]{0,1:T(8,128)(2,1)} async-done(((bf16[1536,96]{0,1:T(8,128)(2,1)}), bf16[1536,1536]{0,1:T(8,128)(2,1)}) %all-gather.7.cloned.1.call-update) | async-done | bytes 4718608 | tf_op jit(solution)/shard_map/all_gather | solution.py:178
  92.6 6.7 %copy.101 = bf16[1536,1536]{1,0:T(8,128)(2,1)} copy(bf16[1536,1536]{0,1:T(8,128)(2,1)} %all-gather.7.cloned.1.call-done) | data formatting | bytes 9437184 | tf_op jit(solution)/shard_map/all_gather | solution.py:178
  99.3 0.0 all-gather.13.cloned.1.call-start
  99.3 56.9 %all-gather.11.cloned.1.call-done = bf16[768,1536]{0,1:T(8,128)(2,1)} async-done(((bf16[768,96]{0,1:T(8,128)(2,1)}), bf16[768,1536]{0,1:T(8,128)(2,1)}) %all-gather.11.cloned.1.call-update) | async-done | bytes 2359312 | tf_op jit(solution)/shard_map/all_gather | solution.py:178
  156.3 4.3 %copy.121 = bf16[768,1536]{1,0:T(8,128)(2,1)} copy(bf16[768,1536]{0,1:T(8,128)(2,1)} %all-gather.11.cloned.1.call-done) | data formatting | bytes 4718592 | tf_op jit(solution)/shard_map/all_gather | solution.py:178
  160.6 0.0 all-gather.17.cloned.1.call-start
  160.6 76.5 %all-gather.15.cloned.1.call-done = bf16[768,3072]{0,1:T(8,128)(2,1)} async-done(((bf16[768,192]{0,1:T(8,128)(2,1)}), bf16[768,3072]{0,1:T(8,128)(2,1)}) %all-gather.15.cloned.1.call-update) | async-done | bytes 4718608 | tf_op jit(solution)/shard_map/all_gather | solution.py:178
  237.2 6.6 %copy.122 = bf16[768,3072]{1,0:T(8,128)(2,1)} copy(bf16[768,3072]{0,1:T(8,128)(2,1)} %all-gather.15.cloned.1.call-done) | data formatting | bytes 9437184 | tf_op jit(solution)/shard_map/all_gather | solution.py:178
  243.9 0.8 copy-done.4
  244.7 0.0 copy-done.5
  244.7 0.1 constant_dynamic-slice_fusion.2
  244.8 0.1 copy.124
  244.9 0.1 copy.125
  245.0 1.8 constant_dynamic-slice_fusion
  246.8 0.1 copy.107
  246.9 0.3 reshape.84
  247.2 0.1 fusion.41
  247.3 0.6 maximum_bitcast_fusion.1
  247.9 0.2 fusion.27
  248.1 0.2 fusion.39
  248.3 1.2 add_bitcast_fusion
  249.5 9.4 %all-gather.9.cloned.1.call-done = bf16[3072,1536]{1,0:T(8,128)(2,1)} async-done(((bf16[1536,1536]{1,0:T(8,128)(2,1)}), bf16[3072,1536]{1,0:T(8,128)(2,1)}) %all-gather.9.cloned.1.call-update) | async-done | bytes 9437200 | tf_op jit(solution)/shard_map/all_gather | solution.py:179
  258.9 5.1 %fusion.15 = bf16[2,64,1536]{2,1,0:T(8,128)(2,1)S(1)} fusion(bf16[3072,1536]{1,0:T(8,128)(2,1)} %all-gather.9.cloned.1.call-done, bf16[2,64,3072]{2,1,0:T(8,128)(2,1)S(1)} %copy-done, f32[3072]{0:T(1024)S(1)} %copy-done.3, f32[2,64]{1,0:T(2,128)S(1)} %add_rsqrt_fusion.1), kind=kOutput, calls=%fused_computation.9 | convolution fusion | flops 1209729024 | bytes 10629632 | tf_op jit(solution)/shard_map/std,dw->stw/dot_general | solution.py:200
  264.0 2.6 reshape.81
  266.6 2.6 copy.102
  269.2 2.2 copy.103
  271.4 6.8 %all-to-all-start = ((bf16[96,2,4,256]{3,2,1,0:T(4,128)(2,1)}), bf16[96,2,4,256]{3,2,1,0:T(4,128)(2,1)S(1)}, u32[]{:S(2)}, u32[]{:S(2)}) async-start(bf16[96,2,4,256]{3,2,1,0:T(4,128)(2,1)} %copy.103), calls=%async_computation | async-start | bytes 786432 | tf_op jit(solution)/shard_map/all_to_all | solution.py:206
  278.2 0.6 maximum_bitcast_fusion
  278.8 0.1 mul.215
  278.9 0.1 mul.224
  279.0 0.1 copy.115
  279.1 0.1 mul.219
  279.2 0.1 mul.220
  279.3 1.2 copy.109
  280.5 0.7 reshape.85.b_re
  281.2 0.2 copy.110
  281.4 0.7 reshape.86.b_im
  282.1 0.1 copy.111
  282.2 0.2 reshape.87
  282.4 0.1 copy.112
  282.4 0.7 reshape.88.c_re
  283.2 0.1 copy.113
  283.2 0.7 reshape.89.c_im
  284.0 0.1 reshape.90
  284.1 0.7 tile.13.skip
  284.8 1.4 fusion.37
  286.1 5.1 %tables.1 = (bf16[6,256,256]{2,1,0:T(8,128)(2,1)}, bf16[6,256,256]{2,1,0:T(8,128)(2,1)}, bf16[6,256,256]{2,1,0:T(8,128)(2,1)}) custom-call(f32[6,16,128]{2,1,0:T(8,128)} %reshape.85.b_re, f32[6,16,128]{2,1,0:T(8,128)} %reshape.86.b_im, f32[6,16,128]{2,1,0:T(8,128)} %reshape.88.c_re, f32[6,16,128]{2,1,0:T(8,128)} %reshape.89.c_im, ...), custom_call_target="tpu_custom_call" | custom-call | flops 1610612736 | bytes 2359296 | tf_op jit(solution)/shard_map/tables/pallas_call | solution.py:102
  291.2 0.2 copy.104
  291.4 0.8 reshape.83.u_ref
  292.3 6.4 %mixer.1 = bf16[6,128,256]{2,1,0:T(8,128)(2,1)} custom-call(bf16[6,128,256]{2,1,0:T(8,128)(2,1)} %reshape.83.u_ref, bf16[6,256,256]{2,1,0:T(8,128)(2,1)} %get-tuple-element.8.within, bf16[6,256,256]{2,1,0:T(8,128)(2,1)} %get-tuple-element.9.enter, bf16[6,256,256]{2,1,0:T(8,128)(2,1)} %get-tuple-element.10.leave, f32[6,54,128]{2,1,0:T(8,128)} %get-tuple-element.16.p_re, ...), custom_call_target="tpu_custom_call" | custom-call | tf_op jit(solution)/shard_map/mixer/pallas_call | solution.py:153
  298.6 1.4 copy.117
  300.0 19.2 %all_to_all.30 = bf16[6,2,64,256]{3,1,0,2:T(2,128)(2,1)S(1)} all-to-all(bf16[6,2,64,256]{3,1,0,2:T(2,128)(2,1)S(1)} %copy.117), channel_id=1, replica_groups=mesh['sp'=16,'dp'=2] {'sp'}, dimensions={2} | all-to-all | bytes 786432 | tf_op jit(solution)/shard_map/all_to_all | solution.py:212
  319.2 0.2 copy.119
  319.4 2.1 reshape.92
  321.5 3.7 %copy.120 = bf16[2,4,16,96,16]{4,3,2,1,0:T(8,128)(2,1)} copy(bf16[2,4,16,96,16]{4,2,1,0,3:T(8,128)(2,1)S(1)} %bitcast.85) | data formatting | bytes 786432 | tf_op jit(solution)/shard_map/transpose | solution.py:214
  325.2 6.2 %reshape.93 = bf16[2,64,1536]{2,1,0:T(8,128)(2,1)S(1)} reshape(bf16[2,4,16,96,16]{4,3,2,1,0:T(8,128)(2,1)} %copy.120) | data formatting | bytes 786432 | tf_op jit(solution)/shard_map/reshape | solution.py:214
  331.5 7.3 %multiply_reduce_fusion = (f32[2,64]{1,0:T(2,128)S(1)}, f32[2,64,3072]{2,1,0:T(8,128)S(1)}) fusion(bf16[1536,3072]{1,0:T(8,128)(2,1)} %all-gather.17.cloned.1.call-done, bf16[2,64,1536]{2,1,0:T(8,128)(2,1)S(1)} %reshape.93, bf16[1536,1536]{1,0:T(8,128)(2,1)} %all-gather.13.cloned.1.call-done), kind=kOutput, calls=%fused_computation.19 | convolution fusion | flops 1813905280 | bytes 16122368 | tf_op jit(solution)/shard_map/stw,wd->std/dot_general | solution.py:217
  338.8 1.1 multiply_convert_fusion
  (35 shorter events, 0.2 us)
Async XLA Ops:
  6.5 86.0 %all-gather.7.cloned.1.call-start = ((), (), s32[]{:S(2)}) async-start(), calls=%async_computation.2 | async-start | bytes 5013504 | tf_op jit(solution)/shard_map/all_gather | solution.py:178
  7.3 149.0 %all-gather.11.cloned.1.call-start = ((), (), s32[]{:S(2)}) async-start(), calls=%async_computation.4 | async-start | bytes 2506752 | tf_op jit(solution)/shard_map/all_gather | solution.py:178
  8.0 229.1 %all-gather.15.cloned.1.call-start = ((), (), s32[]{:S(2)}) async-start(), calls=%async_computation.6 | async-start | bytes 5013504 | tf_op jit(solution)/shard_map/all_gather | solution.py:178
  8.7 250.2 %all-gather.9.cloned.1.call-start = ((), (), s32[]{:S(2)}) async-start(), calls=%async_computation.3 | async-start | bytes 14155776 | tf_op jit(solution)/shard_map/all_gather | solution.py:179
  99.3 232.2 %all-gather.13.cloned.1.call-start = ((), (), s32[]{:S(2)}) async-start(), calls=%async_computation.5 | async-start | bytes 7077888 | tf_op jit(solution)/shard_map/all_gather | solution.py:179
  160.6 170.9 %all-gather.17.cloned.1.call-start = ((), (), s32[]{:S(2)}) async-start(), calls=%async_computation.7 | async-start | bytes 14155776 | tf_op jit(solution)/shard_map/all_gather | solution.py:179
  243.8 0.9 copy-start.4
  243.8 0.9 copy-start.5
  243.8 3.4 copy-start.8
  243.8 4.1 %copy-start = (bf16[2,64,3072]{2,1,0:T(8,128)(2,1)S(1)}, bf16[2,64,3072]{2,1,0:T(8,128)(2,1)}, u32[]{:S(2)}) copy-start(bf16[2,64,3072]{2,1,0:T(8,128)(2,1)} %param.12) | copy-start | bytes 2359300
  243.8 15.1 %copy-start.3 = (f32[3072]{0:T(1024)S(1)}, f32[3072]{0:T(1024)}, u32[]{:S(2)}) copy-start(f32[3072]{0:T(1024)} %param.13) | copy-start | bytes 36868
  266.6 14.6 %copy-start.1 = (f32[6,16,2,64]{1,3,0,2:T(8,128)S(1)}, f32[6,16,2,64]{1,3,0,2:T(8,128)}, u32[]{:S(2)}) copy-start(f32[6,16,2,64]{1,3,0,2:T(8,128)} %get-tuple-element.11) | copy-start | bytes 147460
  269.2 12.9 %copy-start.2 = (f32[2,2,6,1024]{3,2,1,0:T(8,128)S(1)}, f32[2,2,6,1024]{3,2,1,0:T(8,128)}, u32[]{:S(2)}) copy-start(f32[2,2,6,1024]{3,2,1,0:T(8,128)} %get-tuple-element.25) | copy-start | bytes 294916
  269.2 14.8 %copy-start.7 = (f32[1536]{0:T(1024)S(1)}, f32[1536]{0:T(1024)}, u32[]{:S(2)}) copy-start(f32[1536]{0:T(1024)} %param.20) | copy-start | bytes 18436
  271.4 19.9 %all-to-all-start = ((bf16[96,2,4,256]{3,2,1,0:T(4,128)(2,1)}), bf16[96,2,4,256]{3,2,1,0:T(4,128)(2,1)S(1)}, u32[]{:S(2)}, u32[]{:S(2)}) async-start(bf16[96,2,4,256]{3,2,1,0:T(4,128)(2,1)} %copy.103), calls=%async_computation | async-start | bytes 786432 | tf_op jit(solution)/shard_map/all_to_all | solution.py:206
  331.4 7.4 %copy-start.6 = (f32[3072]{0:T(1024)S(1)}, f32[3072]{0:T(1024)}, u32[]{:S(2)}) copy-start(f32[3072]{0:T(1024)} %param.23) | copy-start | bytes 36868
Sparse Core Ops, SparseCore 0:
  10.1 82.3 all-gather.6
  95.4 60.8 all-gather.10
  159.1 78.0 all-gather.14
  238.6 20.2 all-gather.8
  260.3 15.5 all-gather.12
  277.3 22.7 all-gather.16

commit v2 on v1

--- a/solution.py
+++ b/solution.py
@@ -54,6 +54,157 @@
     return b_re, b_im, c_re, c_im, lanes(size * jnp.cos(angle)), lanes(size * jnp.sin(angle))
 
 
+MESH = pl.DeviceIdType.MESH
+
+
+def gather_kernel(sp, dp, shard, out, own_sem, send_sem, recv_sem, pass_sem, take_sem):
+    rows, depth = shard.shape
+    n_y, n_x = 2, 2
+    n_z = sp // (n_y * n_x)
+    me, core = lax.axis_index("sp"), lax.axis_index("dp")
+    z, y, x = me // (n_y * n_x), (me // n_x) % n_y, me % n_x
+    first = (rows // 2 + 15) // 16 * 16
+    halves = ((0, first), (first, rows - first))
+
+    def index(z_at, y_at, x_at):
+        return (z_at * n_y + y_at) * n_x + x_at
+
+    y_other, x_other = (y + 1) % n_y, (x + 1) % n_x
+    y_peer, x_peer = index(z, y_other, x), index(z, y, x_other)
+    z_peers = [index((z + hop) % n_z, y, x) for hop in range(1, n_z)]
+    cores = [(core + hop) % dp for hop in range(1, dp)]
+    barrier = pltpu.get_barrier_semaphore()
+    for peer in [y_peer, x_peer] + z_peers:
+        pl.semaphore_signal(barrier, inc=1, device_id={"sp": peer}, device_id_type=MESH)
+    for peer in cores:
+        pl.semaphore_signal(barrier, inc=1, device_id={"dp": peer}, device_id_type=MESH)
+    pl.semaphore_wait(barrier, 2 + len(z_peers) + len(cores))
+
+    sent, passed = [], []
+
+    def place(who, half, column):
+        start, size = halves[half]
+        return out.at[
+            pl.ds(pl.multiple_of(who * rows + start, 16), size),
+            pl.ds(pl.multiple_of(column * depth, 128), depth),
+        ]
+
+    def source(who, half, mine):
+        return shard.at[pl.ds(*halves[half]), :] if mine else place(who, half, core)
+
+    def send(who, half, peer, mine=False):
+        copy = pltpu.make_async_remote_copy(
+            src_ref=source(who, half, mine),
+            dst_ref=place(who, half, core),
+            send_sem=send_sem.at[len(sent)],
+            recv_sem=recv_sem.at[who, half],
+            device_id={"sp": peer},
+            device_id_type=MESH,
+        )
+        copy.start()
+        sent.append(copy)
+
+    def spread(who, half, mine=False):
+        for hop, peer in enumerate(cores):
+            copy = pltpu.make_async_remote_copy(
+                src_ref=source(who, half, mine),
+                dst_ref=place(who, half, core),
+                send_sem=pass_sem.at[len(passed)],
+                recv_sem=take_sem.at[hop, who, half],
+                device_id={"dp": peer},
+                device_id_type=MESH,
+            )
+            copy.start()
+            passed.append(copy)
+
+    def arrived(who, half):
+        pltpu.make_async_remote_copy(
+            src_ref=place(who, half, core),
+            dst_ref=place(who, half, core),
+            send_sem=send_sem.at[0],
+            recv_sem=recv_sem.at[who, half],
+            device_id={"sp": y_peer},
+            device_id_type=MESH,
+        ).wait_recv()
+
+    own = [
+        pltpu.make_async_copy(source(me, half, True), place(me, half, core), own_sem.at[half])
+        for half in range(2)
+    ]
+    send(me, 0, y_peer, True)
+    send(me, 1, x_peer, True)
+    for peer in z_peers:
+        send(me, 0, peer, True)
+        send(me, 1, peer, True)
+    send(me, 0, x_peer, True)
+    send(me, 1, y_peer, True)
+    for half in range(2):
+        own[half].start()
+        spread(me, half, True)
+    for hop in range(n_z):
+        at = (z + n_z - hop) % n_z
+        if hop > 0:
+            here = index(at, y, x)
+            arrived(here, 0)
+            send(here, 0, y_peer)
+            arrived(here, 1)
+            send(here, 1, x_peer)
+            send(here, 0, x_peer)
+            send(here, 1, y_peer)
+            spread(here, 0)
+            spread(here, 1)
+        by_y, by_x = index(at, y_other, x), index(at, y, x_other)
+        arrived(by_y, 0)
+        send(by_y, 0, x_peer)
+        spread(by_y, 0)
+        arrived(by_x, 1)
+        send(by_x, 1, y_peer)
+        spread(by_x, 1)
+    for hop in range(n_z):
+        at = (z + n_z - hop) % n_z
+        by_y, by_x = index(at, y_other, x), index(at, y, x_other)
+        across = index(at, y_other, x_other)
+        for who, half in ((by_x, 0), (by_y, 1), (across, 0), (across, 1)):
+            arrived(who, half)
+            spread(who, half)
+    for hop in range(1, dp):
+        column = (core + dp - hop) % dp
+        for who in range(sp):
+            for half in range(2):
+                pltpu.make_async_remote_copy(
+                    src_ref=place(who, half, column),
+                    dst_ref=place(who, half, column),
+                    send_sem=pass_sem.at[0],
+                    recv_sem=take_sem.at[hop - 1, who, half],
+                    device_id={"dp": cores[0]},
+                    device_id_type=MESH,
+                ).wait_recv()
+    for copy in own:
+        copy.wait()
+    for copy in sent + passed:
+        copy.wait_send()
+
+
+def relay_gather(shard, sp, dp):
+    rows, depth = shard.shape
+    return pl.pallas_call(
+        functools.partial(gather_kernel, sp, dp),
+        out_shape=jax.ShapeDtypeStruct((sp * rows, dp * depth), shard.dtype),
+        in_specs=[pl.BlockSpec(memory_space=pltpu.VMEM)],
+        out_specs=pl.BlockSpec(memory_space=pl.ANY),
+        scratch_shapes=[
+            pltpu.SemaphoreType.DMA((2,)),
+            pltpu.SemaphoreType.DMA((8 * sp,)),
+            pltpu.SemaphoreType.DMA((sp, 2)),
+            pltpu.SemaphoreType.DMA((2 * sp * (dp - 1),)),
+            pltpu.SemaphoreType.DMA((dp - 1, sp, 2)),
+        ],
+        compiler_params=pltpu.CompilerParams(collective_id=1, has_side_effects=True),
+        cost_estimate=pl.CostEstimate(flops=10**8, bytes_accessed=sp * rows * dp * depth * 2, transcendentals=0),
+        name="relay_gather",
+    )(shard)
+
+
 def table_kernel(b_re, b_im, c_re, c_im, p_re, p_im, within, enter, leave, inner_ref):
     channels, lanes = b_re.shape[1:]
     bre, bim, cre, cim = b_re[0], b_im[0], c_re[0], c_im[0]
@@ -174,10 +325,6 @@
     up_weight,
     post_gain,
 ):
-    def gather(weight):
-        columns = lax.all_gather(weight, "sp", axis=1, tiled=True)
-        return lax.all_gather(columns, "dp", axis=0, tiled=True)
-
     seqs, local_len, _ = tokens.shape
     sp = lax.axis_size("sp")
     group_size = input_matrix.shape[-1] // decay_rate.shape[2]
@@ -188,7 +335,16 @@
     length = near * sp
     offset = lax.axis_index("sp") * own
 
-    in_full = gather(in_weight)
+    dp = lax.axis_size("dp")
+    packed = jnp.concatenate([glu_weight.T, up_weight.T], axis=0)
+    glu_rows, packed_rows = glu_weight.shape[1], packed.shape[0]
+    depth = packed.shape[1]
+    packed = lax.all_gather(packed, "sp", axis=0, tiled=True)
+    packed = lax.all_gather(packed, "dp", axis=0, tiled=True)
+    packed = packed.reshape(dp, sp, packed_rows, depth)
+    glu_full = packed[:, :, :glu_rows].reshape(dp, -1, depth)
+    up_full = packed[:, :, glu_rows:].reshape(dp, -1, depth)
+    in_full = relay_gather(in_weight.T, sp, dp)
     tables = own_tables(
         decay_rate, frequency, log_step, input_matrix, output_matrix, offset, own,
         max(1, (length - 1).bit_length()),
@@ -198,9 +354,8 @@
     skip_rows = jnp.tile(skip_rows, (1, 1, BLOCK))
     normed = rms_scale(tokens, pre_gain).astype(jnp.bfloat16)
     mixer_in = jnp.einsum(
-        "std,dw->stw", normed, in_full, preferred_element_type=jnp.float32
+        "std,wd->stw", normed, in_full, preferred_element_type=jnp.float32
     ).astype(jnp.bfloat16)
-    glu_full, up_full = gather(glu_weight), gather(up_weight)
     blocks = mixer_in.reshape(seqs, near, BLOCK, groups, group_size)
     blocks = jnp.transpose(blocks, (3, 0, 1, 2, 4)).reshape(groups, seqs, near, side)
     blocks = lax.all_to_all(blocks, "sp", split_axis=0, concat_axis=2, tiled=True)
@@ -212,9 +367,19 @@
     mixed = lax.all_to_all(mixed, "sp", split_axis=2, concat_axis=0, tiled=True)
     mixed = mixed.reshape(groups, seqs, near, BLOCK, group_size)
     mixed = jnp.transpose(mixed, (1, 2, 3, 0, 4)).reshape(seqs, local_len, groups * group_size)
-    gate_pre = jnp.einsum("stw,wv->stv", mixed, glu_full, preferred_element_type=jnp.float32)
+    def project(rows, weight):
+        parts = [
+            jnp.einsum(
+                "stw,vw->stv", rows[..., k * depth : (k + 1) * depth], weight[k],
+                preferred_element_type=jnp.float32,
+            )
+            for k in range(dp)
+        ]
+        return functools.reduce(jnp.add, parts)
+
+    gate_pre = project(mixed, glu_full)
     gated = (mixed.astype(jnp.float32) * jax.nn.sigmoid(gate_pre)).astype(jnp.bfloat16)
-    projected = jnp.einsum("stw,wd->std", gated, up_full, preferred_element_type=jnp.float32)
+    projected = project(gated, up_full)
     return rms_scale(projected, post_gain).astype(jnp.bfloat16)
 
 

time: 348 us -> 265 us (0.76)
  waiting for transfers between devices: 229 us -> 105 us
  Pallas kernels: 11.4 us -> 59.3 us
  local copies, waits for them, and re-layouts: 48.8 us -> 37.7 us
    all_gather x6 -> x2, waiting for transfers between devices: 227 us -> 105 us  [the longest x1 105 us: per_device(): packed = lax.all_gather(packed, 'sp', axis=0, tiled=True)]
    pallas_call x0 -> x1, Pallas kernels: none -> 48.4 us  [relay_gather(): pl.pallas_call(functools.partial(gather_kernel, sp, dp), out_shape=jax.Sh...]
    all_gather x3 -> x0, local copies, waits for them, and re-layouts: 17.6 us -> none  [gather(): columns = lax.all_gather(weight, 'sp', axis=1, tiled=True)]
    slice x0 -> x2, local copies, waits for them, and re-layouts: none -> 9.19 us  [project(): weight[k]]
    dot_general x2 -> x5, matrix products: 12.5 us -> 13.9 us  [the longest x4 6.99 us: project(): jnp.einsum('stw,vw->stv', rows[..., k * depth:(k + 1) * depth], weight[k]...]
  transfers between devices with their start and end apart: 7 -> 3, of which waited for: 4 -> 1; matrix products, arithmetic and copies ran while one was open for 16% -> 14% of each run, Pallas kernels for 3% -> 22%
where the time goes in v2:
time: 265 us; the launch traced here: 264 us
  waiting for transfers between devices  105 us (40%)
  Pallas kernels  59.3 us (22%)
  local copies, waits for them, and re-layouts  37.7 us (14%)
  blocking collectives  19.4 us (7%)
  matrix products  13.9 us (5%)
  between operations  13.7 us (5%)
  starting transfers between devices  9.53 us (4%)
  other arithmetic  5.07 us (2%)
    all_gather x1, waiting for transfers between devices, per_device(): packed = lax.all_gather(packed, 'sp', axis=0, tiled=True)  105 us
    pallas_call x1, Pallas kernels, relay_gather(): pl.pallas_call(functools.partial(gather_kernel, sp, dp), out_shape=jax.Sh...  48.4 us
    all_to_all x1, blocking collectives, per_device(): mixed = lax.all_to_all(mixed, 'sp', split_axis=2, concat_axis=0, tiled=True)  19.4 us
    all_to_all x1, starting transfers between devices, per_device(): lax.all_to_all(blocks, 'sp', split_axis=0, concat_axis=2, tiled=True)  9.48 us
    slice x2, local copies, waits for them, and re-layouts, project(): weight[k]  9.19 us
    dot_general x4, matrix products, project(): jnp.einsum('stw,vw->stv', rows[..., k * depth:(k + 1) * depth], weight[k]...  6.99 us
    dot_general x1, matrix products, per_device(): jnp.einsum('std,wd->stw', normed, in_full, preferred_element_type=jnp.flo...  6.93 us
    reshape x1, local copies, waits for them, and re-layouts, per_device(): jnp.transpose(mixed, (1, 2, 3, 0, 4))  6.15 us
  transfers between devices with their start and end apart: 3, of which 1 were waited for; matrix products, arithmetic and copies ran while one was open for 14% of the time, Pallas kernels for 22%

profile of v2, /device:TPU:0, one launch (start us, length us, event | category | flops | bytes accessed | tf_op | source)
XLA Modules:
  0.0 263.8 jit_solution(582601465324245317)
XLA Ops:
  6.5 1.8 pad_maximum_fusion
  8.3 0.0 all-gather.3.cloned.1.call-update
  8.4 0.0 all-gather.5.cloned.1.call-start
  8.4 105.1 %all-gather.3.cloned.1.call-done = bf16[4608,768]{1,0:T(8,128)(2,1)} async-done(((bf16[288,768]{1,0:T(8,128)(2,1)}), bf16[4608,768]{1,0:T(8,128)(2,1)}) %all-gather.3.cloned.1.call-update) | async-done | bytes 7077904 | tf_op jit(solution)/shard_map/all_gather | solution.py:342
  113.5 0.0 all-gather.5.cloned.1.call-update
  113.5 0.0 copy-start
  113.5 0.0 copy-start.4
  113.5 48.4 %relay_gather.1 = bf16[1536,3072]{1,0:T(8,128)(2,1)} custom-call(bf16[96,1536]{1,0:T(8,128)(2,1)} %bitcast.91), custom_call_target="tpu_custom_call" | custom-call | flops 100000000 | bytes 9437184 | tf_op jit(solution)/shard_map/relay_gather/pallas_call | solution.py:190
  161.9 0.2 fusion.11
  162.1 6.9 %fusion.8 = bf16[2,64,1536]{2,1,0:T(8,128)(2,1)S(1)} fusion(bf16[1536,3072]{1,0:T(8,128)(2,1)} %relay_gather.1, bf16[2,64,3072]{2,1,0:T(8,128)(2,1)S(1)} %copy-done, f32[3072]{0:T(1024)S(1)} %copy-done.4, f32[2,64]{1,0:T(2,128)S(1)} %add_rsqrt_fusion.1), kind=kOutput, calls=%fused_computation.10 | convolution fusion | flops 1209729024 | bytes 10629632 | tf_op jit(solution)/shard_map/std,wd->stw/dot_general | solution.py:356
  169.1 2.6 reshape.94
  171.7 0.0 copy-start.2
  171.7 0.0 copy-start.3
  171.7 2.6 copy.88
  174.3 2.1 copy.89
  176.4 9.5 %all-to-all-start = ((bf16[96,2,4,256]{3,2,1,0:T(4,128)(2,1)}), bf16[96,2,4,256]{3,2,1,0:T(4,128)(2,1)S(1)}, u32[]{:S(2)}, u32[]{:S(2)}) async-start(bf16[96,2,4,256]{3,2,1,0:T(4,128)(2,1)} %copy.89), calls=%async_computation | async-start | bytes 786432 | tf_op jit(solution)/shard_map/all_to_all | solution.py:361
  185.9 0.1 constant_dynamic-slice_fusion.2
  186.0 0.1 copy.108
  186.1 0.1 copy.109
  186.2 1.1 constant_dynamic-slice_fusion
  187.3 0.1 copy.93
  187.3 0.3 reshape.97
  187.7 0.1 fusion.28
  187.8 0.1 maximum_bitcast_fusion.1
  187.9 0.2 fusion.26
  188.0 0.0 copy-start.6
  188.0 0.3 add_bitcast_fusion
  188.3 0.1 mul.215
  188.4 0.1 mul.224
  188.5 0.1 copy.101
  188.6 0.1 mul.219
  188.7 0.1 mul.220
  188.8 0.2 copy.95
  189.0 0.7 reshape.98.b_re
  189.7 0.2 copy.96
  189.9 0.7 reshape.99.b_im
  190.6 0.1 copy.97
  190.7 0.2 reshape.100
  190.9 0.1 copy.98
  191.0 0.7 reshape.101.c_re
  191.7 0.1 copy.99
  191.8 0.7 reshape.102.c_im
  192.5 0.1 reshape.103
  192.6 0.7 tile.13.skip
  193.3 1.4 fusion.24
  194.7 4.9 %tables.1 = (bf16[6,256,256]{2,1,0:T(8,128)(2,1)}, bf16[6,256,256]{2,1,0:T(8,128)(2,1)}, bf16[6,256,256]{2,1,0:T(8,128)(2,1)}) custom-call(f32[6,16,128]{2,1,0:T(8,128)} %reshape.98.b_re, f32[6,16,128]{2,1,0:T(8,128)} %reshape.99.b_im, f32[6,16,128]{2,1,0:T(8,128)} %reshape.101.c_re, f32[6,16,128]{2,1,0:T(8,128)} %reshape.102.c_im, ...), custom_call_target="tpu_custom_call" | custom-call | flops 1610612736 | bytes 2359296 | tf_op jit(solution)/shard_map/tables/pallas_call | solution.py:253
  199.6 0.2 copy.90
  199.8 0.9 reshape.96.u_ref
  200.6 6.1 %mixer.1 = bf16[6,128,256]{2,1,0:T(8,128)(2,1)} custom-call(bf16[6,128,256]{2,1,0:T(8,128)(2,1)} %reshape.96.u_ref, bf16[6,256,256]{2,1,0:T(8,128)(2,1)} %get-tuple-element.8.within, bf16[6,256,256]{2,1,0:T(8,128)(2,1)} %get-tuple-element.9.enter, bf16[6,256,256]{2,1,0:T(8,128)(2,1)} %get-tuple-element.10.leave, f32[6,54,128]{2,1,0:T(8,128)} %get-tuple-element.20.p_re, ...), custom_call_target="tpu_custom_call" | custom-call | tf_op jit(solution)/shard_map/mixer/pallas_call | solution.py:304
  206.7 1.4 copy.103
  208.1 19.4 %all_to_all.30 = bf16[6,2,64,256]{3,1,0,2:T(2,128)(2,1)S(1)} all-to-all(bf16[6,2,64,256]{3,1,0,2:T(2,128)(2,1)S(1)} %copy.103), channel_id=1, replica_groups=mesh['sp'=16,'dp'=2] {'sp'}, dimensions={2} | all-to-all | bytes 786432 | tf_op jit(solution)/shard_map/all_to_all | solution.py:367
  227.4 0.2 copy.105
  227.6 2.1 reshape.105
  229.7 3.6 %copy.106 = bf16[2,4,16,96,16]{4,3,2,1,0:T(8,128)(2,1)} copy(bf16[2,4,16,96,16]{4,2,1,0,3:T(8,128)(2,1)S(1)} %bitcast.84) | data formatting | bytes 786432 | tf_op jit(solution)/shard_map/transpose | solution.py:369
  233.4 6.2 %reshape.106 = bf16[2,64,1536]{2,1,0:T(8,128)(2,1)S(1)} reshape(bf16[2,4,16,96,16]{4,3,2,1,0:T(8,128)(2,1)} %copy.106) | data formatting | bytes 786432 | tf_op jit(solution)/shard_map/reshape | solution.py:369
  239.5 0.0 all-gather.5.cloned.1.call-done
  239.6 4.8 %fusion.30 = (bf16[1,16,96,768]{3,2,1,0:T(8,128)(2,1)}, bf16[1,16,96,768]{3,2,1,0:T(8,128)(2,1)}) fusion(bf16[2,16,288,768]{3,2,1,0:T(8,128)(2,1)} %bitcast.81), kind=kLoop, calls=%fused_computation.66 | loop fusion | bytes 9437184 | tf_op jit(solution)/shard_map/slice | solution.py:373
  244.4 4.4 %fusion.29 = (bf16[1,16,192,768]{3,2,1,0:T(8,128)(2,1)S(1)}, bf16[1,16,192,768]{3,2,1,0:T(8,128)(2,1)S(1)}) fusion(bf16[2,16,288,768]{3,2,1,0:T(8,128)(2,1)} %bitcast.82), kind=kLoop, calls=%fused_computation.65 | loop fusion | bytes 18874368 | tf_op jit(solution)/shard_map/slice | solution.py:373
  248.8 2.7 %fusion.21 = f32[2,64,1536]{2,1,0:T(8,128)S(1)} fusion(bf16[1536,768,1]{1,0,2:T(8,128)(2,1)} %bitcast.85, bf16[2,64,1536]{2,1,0:T(8,128)(2,1)S(1)} %reshape.106), kind=kOutput, calls=%fused_computation.31 | convolution fusion | flops 301989888 | bytes 3342336 | tf_op jit(solution)/shard_map/stw,vw->stv/dot_general | solution.py:372
  251.5 1.0 fusion.7
  252.4 1.6 fusion.18
  254.1 0.0 copy-start.5
  254.1 1.7 multiply_reduce_fusion
  255.8 1.1 multiply_convert_fusion
  (25 shorter events, 0.1 us)
Async XLA Ops:
  6.5 106.9 %all-gather.3.cloned.1.call-start = ((), (), s32[]{:S(2)}) async-start(), calls=%async_computation.2 | async-start | bytes 7520256 | tf_op jit(solution)/shard_map/all_gather | solution.py:342
  8.4 231.2 %all-gather.5.cloned.1.call-start = ((), (), s32[]{:S(2)}) async-start(), calls=%async_computation.3 | async-start | bytes 21233664 | tf_op jit(solution)/shard_map/all_gather | solution.py:343
  113.5 48.4 %copy-start = (bf16[2,64,3072]{2,1,0:T(8,128)(2,1)S(1)}, bf16[2,64,3072]{2,1,0:T(8,128)(2,1)}, u32[]{:S(2)}) copy-start(bf16[2,64,3072]{2,1,0:T(8,128)(2,1)} %param.12) | copy-start | bytes 2359300
  113.5 48.6 %copy-start.4 = (f32[3072]{0:T(1024)S(1)}, f32[3072]{0:T(1024)}, u32[]{:S(2)}) copy-start(f32[3072]{0:T(1024)} %param.13) | copy-start | bytes 36868
  171.7 14.2 %copy-start.2 = (f32[2,96,64]{1,2,0:T(8,128)S(1)}, f32[2,96,64]{1,2,0:T(8,128)}, u32[]{:S(2)}) copy-start(f32[2,96,64]{1,2,0:T(8,128)} %param.16) | copy-start | bytes 147460
  171.7 14.2 %copy-start.3 = (f32[2,96,64]{1,2,0:T(8,128)S(1)}, f32[2,96,64]{1,2,0:T(8,128)}, u32[]{:S(2)}) copy-start(f32[2,96,64]{1,2,0:T(8,128)} %param.15) | copy-start | bytes 147460
  174.3 13.4 %copy-start.7 = (f32[2,96]{1,0:T(2,128)S(1)}, f32[2,96]{1,0:T(2,128)}, u32[]{:S(2)}) copy-start(f32[2,96]{1,0:T(2,128)} %param.17) | copy-start | bytes 2308
  176.4 23.2 %all-to-all-start = ((bf16[96,2,4,256]{3,2,1,0:T(4,128)(2,1)}), bf16[96,2,4,256]{3,2,1,0:T(4,128)(2,1)S(1)}, u32[]{:S(2)}, u32[]{:S(2)}) async-start(bf16[96,2,4,256]{3,2,1,0:T(4,128)(2,1)} %copy.89), calls=%async_computation | async-start | bytes 786432 | tf_op jit(solution)/shard_map/all_to_all | solution.py:361
  188.0 4.5 %copy-start.6 = (f32[1536]{0:T(1024)S(1)}, f32[1536]{0:T(1024)}, u32[]{:S(2)}) copy-start(f32[1536]{0:T(1024)} %param.20) | copy-start | bytes 18436
  248.8 2.7 %copy-start.1 = (bf16[1,16,96,768]{3,2,1,0:T(8,128)(2,1)S(1)}, bf16[1,16,96,768]{3,2,1,0:T(8,128)(2,1)}, u32[]{:S(2)}) copy-start(bf16[1,16,96,768]{3,2,1,0:T(8,128)(2,1)} %get-tuple-element.13) | copy-start | bytes 7077892
  254.1 1.8 copy-start.5
Sparse Core Ops, SparseCore 0:
  10.1 103.2 all-gather.2
  115.0 25.5 all-gather.4

commit v3 on v2

--- a/solution.py
+++ b/solution.py
@@ -6,6 +6,7 @@
 from jax.experimental import pallas as pl
 from jax.experimental.pallas import tpu as pltpu
 from jax.sharding import PartitionSpec as P
+
 
 epsilon = 1e-06
 BLOCK = 16
@@ -298,7 +299,7 @@
 
 
 def run_scan(blocks, within, enter, leave, p_re, p_im, skip, length):
-    own, rows, side = blocks.shape
+    own, _, _ = blocks.shape
     whole = lambda value: pl.BlockSpec((1,) + value.shape[1:], lambda g: (g, 0, 0))
     operands = (blocks, within, enter, leave, p_re, p_im, skip)
     return pl.pallas_call(
@@ -363,10 +364,12 @@
         blocks.reshape(own, seqs * length, side), within, enter, leave, tables[4], tables[5],
         skip_rows, length,
     )
-    mixed = mixed.reshape(own, seqs, length, side)
-    mixed = lax.all_to_all(mixed, "sp", split_axis=2, concat_axis=0, tiled=True)
+    mixed = jnp.transpose(mixed.reshape(own, seqs, sp, near, side), (2, 0, 1, 3, 4))
+    mixed = mixed.reshape(groups, seqs, near, side)
+    mixed = lax.all_to_all(mixed, "sp", split_axis=0, concat_axis=0, tiled=True)
     mixed = mixed.reshape(groups, seqs, near, BLOCK, group_size)
     mixed = jnp.transpose(mixed, (1, 2, 3, 0, 4)).reshape(seqs, local_len, groups * group_size)
+
     def project(rows, weight):
         parts = [
             jnp.einsum(

time: 265 us -> 262 us (0.989)
  transfers between devices with their start and end apart: 3 -> 3, of which waited for: 1 -> 1; matrix products, arithmetic and copies ran while one was open for 14% -> 13% of each run, Pallas kernels for 22% -> 23%
where the time goes in v3:
time: 262 us; the launch traced here: 261 us
  waiting for transfers between devices  105 us (40%)
  Pallas kernels  59.3 us (23%)
  local copies, waits for them, and re-layouts  35.3 us (13%)
  blocking collectives  19.4 us (7%)
  matrix products  13.9 us (5%)
  between operations  13.8 us (5%)
  starting transfers between devices  9.53 us (4%)
  other arithmetic  5.07 us (2%)
    all_gather x1, waiting for transfers between devices, per_device(): packed = lax.all_gather(packed, 'sp', axis=0, tiled=True)  105 us
    pallas_call x1, Pallas kernels, relay_gather(): pl.pallas_call(functools.partial(gather_kernel, sp, dp), out_shape=jax.Sh...  48.4 us
    all_to_all x1, blocking collectives, per_device(): mixed = lax.all_to_all(mixed, 'sp', split_axis=0, concat_axis=0, tiled=True)  19.4 us
    all_to_all x1, starting transfers between devices, per_device(): lax.all_to_all(blocks, 'sp', split_axis=0, concat_axis=2, tiled=True)  9.48 us
    slice x2, local copies, waits for them, and re-layouts, project(): weight[k]  9.19 us
    dot_general x4, matrix products, project(): jnp.einsum('stw,vw->stv', rows[..., k * depth:(k + 1) * depth], weight[k]...  7.01 us
    dot_general x1, matrix products, per_device(): jnp.einsum('std,wd->stw', normed, in_full, preferred_element_type=jnp.flo...  6.93 us
    pallas_call x1, Pallas kernels, run_scan(): pl.pallas_call(functools.partial(scan_kernel, length), grid=(own,), out_s...  6.06 us
  transfers between devices with their start and end apart: 3, of which 1 were waited for; matrix products, arithmetic and copies ran while one was open for 13% of the time, Pallas kernels for 23%

profile of v3, /device:TPU:0, one launch (start us, length us, event | category | flops | bytes accessed | tf_op | source)
XLA Modules:
  0.0 261.4 jit_solution(9447871769126215037)
XLA Ops:
  6.5 1.8 pad_maximum_fusion
  8.3 0.0 all-gather.3.cloned.1.call-update
  8.4 0.0 all-gather.5.cloned.1.call-start
  8.4 105.1 %all-gather.3.cloned.1.call-done = bf16[4608,768]{1,0:T(8,128)(2,1)} async-done(((bf16[288,768]{1,0:T(8,128)(2,1)}), bf16[4608,768]{1,0:T(8,128)(2,1)}) %all-gather.3.cloned.1.call-update) | async-done | bytes 7077904 | tf_op jit(solution)/shard_map/all_gather | solution.py:343
  113.5 0.0 all-gather.5.cloned.1.call-update
  113.5 0.0 copy-start
  113.5 0.0 copy-start.4
  113.5 48.4 %relay_gather.1 = bf16[1536,3072]{1,0:T(8,128)(2,1)} custom-call(bf16[96,1536]{1,0:T(8,128)(2,1)} %bitcast.91), custom_call_target="tpu_custom_call" | custom-call | flops 100000000 | bytes 9437184 | tf_op jit(solution)/shard_map/relay_gather/pallas_call | solution.py:191
  161.9 0.2 fusion.11
  162.1 6.9 %fusion.8 = bf16[2,64,1536]{2,1,0:T(8,128)(2,1)S(1)} fusion(bf16[1536,3072]{1,0:T(8,128)(2,1)} %relay_gather.1, bf16[2,64,3072]{2,1,0:T(8,128)(2,1)S(1)} %copy-done, f32[3072]{0:T(1024)S(1)} %copy-done.4, f32[2,64]{1,0:T(2,128)S(1)} %add_rsqrt_fusion.1), kind=kOutput, calls=%fused_computation.10 | convolution fusion | flops 1209729024 | bytes 10629632 | tf_op jit(solution)/shard_map/std,wd->stw/dot_general | solution.py:357
  169.1 2.6 reshape.96
  171.7 0.0 copy-start.2
  171.7 0.0 copy-start.3
  171.7 2.6 copy.70
  174.3 2.1 copy.71
  176.4 9.5 %all-to-all-start = ((bf16[96,2,4,256]{3,2,1,0:T(4,128)(2,1)}), bf16[96,2,4,256]{3,2,1,0:T(4,128)(2,1)S(1)}, u32[]{:S(2)}, u32[]{:S(2)}) async-start(bf16[96,2,4,256]{3,2,1,0:T(4,128)(2,1)} %copy.71), calls=%async_computation | async-start | bytes 786432 | tf_op jit(solution)/shard_map/all_to_all | solution.py:362
  185.9 0.1 constant_dynamic-slice_fusion.2
  186.0 0.1 copy.88
  186.1 0.1 copy.89
  186.2 1.1 constant_dynamic-slice_fusion
  187.3 0.1 copy.75
  187.3 0.3 reshape.99
  187.7 0.1 fusion.28
  187.8 0.1 maximum_bitcast_fusion.1
  187.9 0.2 fusion.26
  188.0 0.0 copy-start.6
  188.0 0.3 add_bitcast_fusion
  188.3 0.1 mul.215
  188.4 0.1 mul.224
  188.5 0.1 copy.83
  188.6 0.1 mul.219
  188.7 0.1 mul.220
  188.8 0.2 copy.77
  189.0 0.7 reshape.100.b_re
  189.7 0.2 copy.78
  189.9 0.7 reshape.101.b_im
  190.6 0.1 copy.79
  190.7 0.2 reshape.102
  190.9 0.1 copy.80
  191.0 0.7 reshape.103.c_re
  191.7 0.1 copy.81
  191.8 0.7 reshape.104.c_im
  192.5 0.1 reshape.105
  192.6 0.7 tile.13.skip
  193.3 1.4 fusion.24
  194.7 4.9 %tables.1 = (bf16[6,256,256]{2,1,0:T(8,128)(2,1)}, bf16[6,256,256]{2,1,0:T(8,128)(2,1)}, bf16[6,256,256]{2,1,0:T(8,128)(2,1)}) custom-call(f32[6,16,128]{2,1,0:T(8,128)} %reshape.100.b_re, f32[6,16,128]{2,1,0:T(8,128)} %reshape.101.b_im, f32[6,16,128]{2,1,0:T(8,128)} %reshape.103.c_re, f32[6,16,128]{2,1,0:T(8,128)} %reshape.104.c_im, ...), custom_call_target="tpu_custom_call" | custom-call | flops 1610612736 | bytes 2359296 | tf_op jit(solution)/shard_map/tables/pallas_call | solution.py:254
  199.6 0.2 copy.72
  199.8 0.9 reshape.98.u_ref
  200.6 6.1 %mixer.1 = bf16[6,128,256]{2,1,0:T(8,128)(2,1)} custom-call(bf16[6,128,256]{2,1,0:T(8,128)(2,1)} %reshape.98.u_ref, bf16[6,256,256]{2,1,0:T(8,128)(2,1)} %get-tuple-element.8.within, bf16[6,256,256]{2,1,0:T(8,128)(2,1)} %get-tuple-element.9.enter, bf16[6,256,256]{2,1,0:T(8,128)(2,1)} %get-tuple-element.10.leave, f32[6,54,128]{2,1,0:T(8,128)} %get-tuple-element.20.p_re, ...), custom_call_target="tpu_custom_call" | custom-call | tf_op jit(solution)/shard_map/mixer/pallas_call | solution.py:305
  206.7 1.1 reshape.106
  207.8 0.1 copy.85
  207.9 19.4 %all_to_all.20 = bf16[96,2,4,256]{3,2,1,0:T(4,128)(2,1)S(1)} all-to-all(bf16[96,2,4,256]{3,2,1,0:T(4,128)(2,1)S(1)} %bitcast.90), channel_id=1, replica_groups=mesh['sp'=16,'dp'=2] {'sp'}, dimensions={0} | all-to-all | bytes 786432 | tf_op jit(solution)/shard_map/all_to_all | solution.py:369
  227.3 1.2 copy.86
  228.4 3.1 %copy.87 = bf16[2,4,16,96,16]{4,3,2,1,0:T(8,128)(2,1)S(1)} copy(bf16[2,4,16,96,16]{3,4,2,1,0:T(8,128)(2,1)} %bitcast.88) | data formatting | bytes 786432 | tf_op jit(solution)/shard_map/transpose | solution.py:371
  231.5 5.6 %reshape.109 = bf16[2,64,1536]{2,1,0:T(8,128)(2,1)S(1)} reshape(bf16[2,4,16,96,16]{4,3,2,1,0:T(8,128)(2,1)S(1)} %copy.87) | data formatting | bytes 786432 | tf_op jit(solution)/shard_map/reshape | solution.py:371
  237.1 0.0 all-gather.5.cloned.1.call-done
  237.2 4.8 %fusion.30 = (bf16[1,16,96,768]{3,2,1,0:T(8,128)(2,1)}, bf16[1,16,96,768]{3,2,1,0:T(8,128)(2,1)}) fusion(bf16[2,16,288,768]{3,2,1,0:T(8,128)(2,1)} %bitcast.82), kind=kLoop, calls=%fused_computation.66 | loop fusion | bytes 9437184 | tf_op jit(solution)/shard_map/slice | solution.py:376
  242.0 4.4 %fusion.29 = (bf16[1,16,192,768]{3,2,1,0:T(8,128)(2,1)S(1)}, bf16[1,16,192,768]{3,2,1,0:T(8,128)(2,1)S(1)}) fusion(bf16[2,16,288,768]{3,2,1,0:T(8,128)(2,1)} %bitcast.83), kind=kLoop, calls=%fused_computation.65 | loop fusion | bytes 18874368 | tf_op jit(solution)/shard_map/slice | solution.py:376
  246.4 2.7 %fusion.21 = f32[2,64,1536]{2,1,0:T(8,128)S(1)} fusion(bf16[1536,768,1]{1,0,2:T(8,128)(2,1)} %bitcast.85, bf16[2,64,1536]{2,1,0:T(8,128)(2,1)S(1)} %reshape.109), kind=kOutput, calls=%fused_computation.31 | convolution fusion | flops 301989888 | bytes 3342336 | tf_op jit(solution)/shard_map/stw,vw->stv/dot_general | solution.py:375
  249.1 0.9 fusion.7
  250.1 1.6 fusion.18
  251.7 0.0 copy-start.5
  251.7 1.7 multiply_reduce_fusion
  253.5 1.1 multiply_convert_fusion
  (25 shorter events, 0.1 us)
Async XLA Ops:
  6.5 106.9 %all-gather.3.cloned.1.call-start = ((), (), s32[]{:S(2)}) async-start(), calls=%async_computation.2 | async-start | bytes 7520256 | tf_op jit(solution)/shard_map/all_gather | solution.py:343
  8.4 228.8 %all-gather.5.cloned.1.call-start = ((), (), s32[]{:S(2)}) async-start(), calls=%async_computation.3 | async-start | bytes 21233664 | tf_op jit(solution)/shard_map/all_gather | solution.py:344
  113.5 48.4 %copy-start = (bf16[2,64,3072]{2,1,0:T(8,128)(2,1)S(1)}, bf16[2,64,3072]{2,1,0:T(8,128)(2,1)}, u32[]{:S(2)}) copy-start(bf16[2,64,3072]{2,1,0:T(8,128)(2,1)} %param.12) | copy-start | bytes 2359300
  113.5 48.6 %copy-start.4 = (f32[3072]{0:T(1024)S(1)}, f32[3072]{0:T(1024)}, u32[]{:S(2)}) copy-start(f32[3072]{0:T(1024)} %param.13) | copy-start | bytes 36868
  171.7 14.2 %copy-start.2 = (f32[2,96,64]{1,2,0:T(8,128)S(1)}, f32[2,96,64]{1,2,0:T(8,128)}, u32[]{:S(2)}) copy-start(f32[2,96,64]{1,2,0:T(8,128)} %param.16) | copy-start | bytes 147460
  171.7 14.2 %copy-start.3 = (f32[2,96,64]{1,2,0:T(8,128)S(1)}, f32[2,96,64]{1,2,0:T(8,128)}, u32[]{:S(2)}) copy-start(f32[2,96,64]{1,2,0:T(8,128)} %param.15) | copy-start | bytes 147460
  174.3 13.4 %copy-start.7 = (f32[2,96]{1,0:T(2,128)S(1)}, f32[2,96]{1,0:T(2,128)}, u32[]{:S(2)}) copy-start(f32[2,96]{1,0:T(2,128)} %param.17) | copy-start | bytes 2308
  176.4 23.2 %all-to-all-start = ((bf16[96,2,4,256]{3,2,1,0:T(4,128)(2,1)}), bf16[96,2,4,256]{3,2,1,0:T(4,128)(2,1)S(1)}, u32[]{:S(2)}, u32[]{:S(2)}) async-start(bf16[96,2,4,256]{3,2,1,0:T(4,128)(2,1)} %copy.71), calls=%async_computation | async-start | bytes 786432 | tf_op jit(solution)/shard_map/all_to_all | solution.py:362
  188.0 4.5 %copy-start.6 = (f32[1536]{0:T(1024)S(1)}, f32[1536]{0:T(1024)}, u32[]{:S(2)}) copy-start(f32[1536]{0:T(1024)} %param.20) | copy-start | bytes 18436
  246.4 2.7 %copy-start.1 = (bf16[1,16,96,768]{3,2,1,0:T(8,128)(2,1)S(1)}, bf16[1,16,96,768]{3,2,1,0:T(8,128)(2,1)}, u32[]{:S(2)}) copy-start(bf16[1,16,96,768]{3,2,1,0:T(8,128)(2,1)} %get-tuple-element.13) | copy-start | bytes 7077892
  251.7 1.8 copy-start.5
Sparse Core Ops, SparseCore 0:
  10.1 103.2 all-gather.2
  115.0 25.5 all-gather.4

commit v4 on v3

--- a/solution.py
+++ b/solution.py
@@ -206,6 +206,37 @@
     )(shard)
 
 
+def swap_kernel(dp, shard, out, send_sem, recv_sem):
+    core = lax.axis_index("dp")
+    barrier = pltpu.get_barrier_semaphore()
+    for hop in range(1, dp):
+        pl.semaphore_signal(barrier, inc=1, device_id={"dp": (core + hop) % dp}, device_id_type=MESH)
+    pl.semaphore_wait(barrier, dp - 1)
+    copies = [
+        pltpu.make_async_remote_copy(
+            src_ref=shard, dst_ref=out.at[hop - 1], send_sem=send_sem.at[hop - 1],
+            recv_sem=recv_sem.at[hop - 1], device_id={"dp": (core + hop) % dp}, device_id_type=MESH,
+        )
+        for hop in range(1, dp)
+    ]
+    for copy in copies:
+        copy.start()
+    for copy in copies:
+        copy.wait()
+
+
+def swap(shard, dp):
+    return pl.pallas_call(
+        functools.partial(swap_kernel, dp),
+        out_shape=jax.ShapeDtypeStruct((dp - 1,) + shard.shape, shard.dtype),
+        in_specs=[pl.BlockSpec(memory_space=pl.ANY)],
+        out_specs=pl.BlockSpec(memory_space=pl.ANY),
+        scratch_shapes=[pltpu.SemaphoreType.DMA((dp - 1,)), pltpu.SemaphoreType.DMA((dp - 1,))],
+        compiler_params=pltpu.CompilerParams(collective_id=2, has_side_effects=True),
+        name="swap",
+    )(shard)
+
+
 def table_kernel(b_re, b_im, c_re, c_im, p_re, p_im, within, enter, leave, inner_ref):
     channels, lanes = b_re.shape[1:]
     bre, bim, cre, cim = b_re[0], b_im[0], c_re[0], c_im[0]
@@ -341,10 +372,12 @@
     glu_rows, packed_rows = glu_weight.shape[1], packed.shape[0]
     depth = packed.shape[1]
     packed = lax.all_gather(packed, "sp", axis=0, tiled=True)
-    packed = lax.all_gather(packed, "dp", axis=0, tiled=True)
-    packed = packed.reshape(dp, sp, packed_rows, depth)
-    glu_full = packed[:, :, :glu_rows].reshape(dp, -1, depth)
-    up_full = packed[:, :, glu_rows:].reshape(dp, -1, depth)
+    core = lax.axis_index("dp")
+    others = swap(packed, dp)
+    held = [packed] + [others[hop] for hop in range(dp - 1)]
+    held = [value.reshape(sp, packed_rows, depth) for value in held]
+    glu_full = [value[:, :glu_rows].reshape(-1, depth) for value in held]
+    up_full = [value[:, glu_rows:].reshape(-1, depth) for value in held]
     in_full = relay_gather(in_weight.T, sp, dp)
     tables = own_tables(
         decay_rate, frequency, log_step, input_matrix, output_matrix, offset, own,
@@ -373,7 +406,7 @@
     def project(rows, weight):
         parts = [
             jnp.einsum(
-                "stw,vw->stv", rows[..., k * depth : (k + 1) * depth], weight[k],
+                "stw,vw->stv", lax.dynamic_slice_in_dim(rows, (core + dp - k) % dp * depth, depth, 2), weight[k],
                 preferred_element_type=jnp.float32,
             )
             for k in range(dp)

time: 262 us -> 203 us (0.77)
  waiting for transfers between devices: 105 us -> 17.4 us
  Pallas kernels: 59.3 us -> 87.4 us
  blocking collectives: 19.4 us -> 0 us
  starting transfers between devices: 9.53 us -> 27.2 us
  local copies, waits for them, and re-layouts: 35.3 us -> 38.4 us
    all_gather x1, waiting for transfers between devices: 105 us -> 0.02 us  [per_device(): packed = lax.all_gather(packed, 'sp', axis=0, tiled=True)]
    all_to_all x1 -> x0, blocking collectives: 19.4 us -> none  [per_device(): mixed = lax.all_to_all(mixed, 'sp', split_axis=0, concat_axis=0, tiled=True)]
    pallas_call x1, Pallas kernels: 48.4 us -> 64.8 us  [relay_gather(): pl.pallas_call(functools.partial(gather_kernel, sp, dp), out_shape=jax.Sh...]
    all_to_all x0 -> x1, waiting for transfers between devices: none -> 12.3 us  [per_device(): mixed = lax.all_to_all(mixed, 'sp', split_axis=0, concat_axis=0, tiled=True)]
    pallas_call x0 -> x1, Pallas kernels: none -> 11.6 us  [swap(): pl.pallas_call(functools.partial(swap_kernel, dp), out_shape=jax.ShapeDty...]
    all_to_all x0 -> x1, starting transfers between devices: none -> 9.14 us  [per_device(): mixed = lax.all_to_all(mixed, 'sp', split_axis=0, concat_axis=0, tiled=True)]
    all_to_all x1, starting transfers between devices: 9.48 us -> 18 us  [per_device(): lax.all_to_all(blocks, 'sp', split_axis=0, concat_axis=2, tiled=True)]
    all_to_all x1, waiting for transfers between devices: 0.01 us -> 5.11 us  [per_device(): lax.all_to_all(blocks, 'sp', split_axis=0, concat_axis=2, tiled=True)]
  transfers between devices with their start and end apart: 3 -> 3, of which waited for: 1 -> 2; matrix products, arithmetic and copies ran while one was open for 13% -> 18% of each run, Pallas kernels for 23% -> 38%
where the time goes in v4:
time: 203 us; the launch traced here: 201 us
  Pallas kernels  87.4 us (43%)
  local copies, waits for them, and re-layouts  38.4 us (19%)
  starting transfers between devices  27.2 us (13%)
  waiting for transfers between devices  17.4 us (9%)
  between operations  13.8 us (7%)
  matrix products  12.2 us (6%)
  other arithmetic  5.09 us (3%)
    pallas_call x1, Pallas kernels, relay_gather(): pl.pallas_call(functools.partial(gather_kernel, sp, dp), out_shape=jax.Sh...  64.8 us
    all_to_all x1, starting transfers between devices, per_device(): lax.all_to_all(blocks, 'sp', split_axis=0, concat_axis=2, tiled=True)  18 us
    all_to_all x1, waiting for transfers between devices, per_device(): mixed = lax.all_to_all(mixed, 'sp', split_axis=0, concat_axis=0, tiled=True)  12.3 us
    pallas_call x1, Pallas kernels, swap(): pl.pallas_call(functools.partial(swap_kernel, dp), out_shape=jax.ShapeDty...  11.6 us
    all_to_all x1, starting transfers between devices, per_device(): mixed = lax.all_to_all(mixed, 'sp', split_axis=0, concat_axis=0, tiled=True)  9.14 us
    slice x2, local copies, waits for them, and re-layouts, per_device(): up_full = [value[:, glu_rows:].reshape(-1, depth) for value in held]  7.74 us
    dot_general x1, matrix products, per_device(): jnp.einsum('std,wd->stw', normed, in_full, preferred_element_type=jnp.flo...  7.04 us
    pallas_call x1, Pallas kernels, run_scan(): pl.pallas_call(functools.partial(scan_kernel, length), grid=(own,), out_s...  6.1 us
  transfers between devices with their start and end apart: 3, of which 2 were waited for; matrix products, arithmetic and copies ran while one was open for 18% of the time, Pallas kernels for 38%

profile of v4, /device:TPU:0, one launch (start us, length us, event | category | flops | bytes accessed | tf_op | source)
XLA Modules:
  0.0 201.5 jit_solution(9626125495387514244)
XLA Ops:
  6.5 1.8 pad_maximum_fusion
  8.3 0.0 all-gather.2.cloned.1.call-update
  8.4 0.0 copy-start
  8.4 0.0 copy-start.3
  8.4 64.8 %relay_gather.1 = bf16[1536,3072]{1,0:T(8,128)(2,1)} custom-call(bf16[96,1536]{1,0:T(8,128)(2,1)} %bitcast.95), custom_call_target="tpu_custom_call" | custom-call | flops 100000000 | bytes 9437184 | tf_op jit(solution)/shard_map/relay_gather/pallas_call | solution.py:191
  73.1 0.2 fusion.11
  73.4 7.0 %fusion.8 = bf16[2,64,1536]{2,1,0:T(8,128)(2,1)S(1)} fusion(bf16[1536,3072]{1,0:T(8,128)(2,1)} %relay_gather.1, bf16[2,64,3072]{2,1,0:T(8,128)(2,1)S(1)} %copy-done, f32[3072]{0:T(1024)S(1)} %copy-done.3, f32[2,64]{1,0:T(2,128)S(1)} %add_rsqrt_fusion.1), kind=kOutput, calls=%fused_computation.10 | convolution fusion | flops 1209729024 | bytes 10629632 | tf_op jit(solution)/shard_map/std,wd->stw/dot_general | solution.py:390
  80.5 2.6 %reshape.98 = bf16[2,4,16,96,16]{4,3,2,1,0:T(8,128)(2,1)S(1)} reshape(bf16[2,64,1536]{2,1,0:T(8,128)(2,1)S(1)} %fusion.8) | data formatting | bytes 786432 | tf_op jit(solution)/shard_map/reshape | solution.py:393
  83.0 0.0 copy-start.1
  83.0 2.6 %copy.70 = bf16[96,2,4,16,16]{0,4,3,2,1:T(8,128)(2,1)} copy(bf16[96,2,4,16,16]{4,0,3,2,1:T(8,128)(2,1)S(1)} %bitcast.89) | data formatting | bytes 786432 | tf_op jit(solution)/shard_map/transpose | solution.py:394
  85.6 2.1 %copy.71 = bf16[96,2,4,256]{3,2,1,0:T(4,128)(2,1)} copy(bf16[96,2,4,256]{0,3,2,1:T(8,128)(2,1)} %bitcast.92) | data formatting | bytes 786432 | tf_op jit(solution)/shard_map/reshape | solution.py:394
  87.7 18.0 %all-to-all-start = ((bf16[96,2,4,256]{3,2,1,0:T(4,128)(2,1)}), bf16[96,2,4,256]{3,2,1,0:T(4,128)(2,1)S(1)}, u32[]{:S(2)}, u32[]{:S(2)}) async-start(bf16[96,2,4,256]{3,2,1,0:T(4,128)(2,1)} %copy.71), calls=%async_computation | async-start | bytes 786432 | tf_op jit(solution)/shard_map/all_to_all | solution.py:395
  105.8 0.1 constant_dynamic-slice_fusion.2
  105.9 0.1 copy.88
  106.0 0.1 copy.89
  106.1 1.1 constant_dynamic-slice_fusion
  107.2 0.1 copy.75
  107.3 0.3 reshape.101
  107.6 0.1 fusion.32
  107.7 0.1 maximum_bitcast_fusion.1
  107.8 0.2 fusion.26
  107.9 0.3 add_bitcast_fusion
  108.2 0.2 copy.77
  108.4 0.7 reshape.102.b_re
  109.1 0.2 copy.78
  109.3 0.7 reshape.103.b_im
  110.0 0.1 mul.223
  110.1 0.1 mul.232
  110.2 0.1 copy.83
  110.3 0.1 mul.227
  110.4 0.1 mul.228
  110.5 0.1 copy.79
  110.6 0.2 reshape.104
  110.8 0.1 copy.80
  110.9 0.7 reshape.105.c_re
  111.6 0.1 copy.81
  111.7 0.7 reshape.106.c_im
  112.4 0.1 reshape.107
  112.5 0.7 tile.13.skip
  113.2 1.4 fusion.24
  114.6 4.9 %tables.1 = (bf16[6,256,256]{2,1,0:T(8,128)(2,1)}, bf16[6,256,256]{2,1,0:T(8,128)(2,1)}, bf16[6,256,256]{2,1,0:T(8,128)(2,1)}) custom-call(f32[6,16,128]{2,1,0:T(8,128)} %reshape.102.b_re, f32[6,16,128]{2,1,0:T(8,128)} %reshape.103.b_im, f32[6,16,128]{2,1,0:T(8,128)} %reshape.105.c_re, f32[6,16,128]{2,1,0:T(8,128)} %reshape.106.c_im, ...), custom_call_target="tpu_custom_call" | custom-call | flops 1610612736 | bytes 2359296 | tf_op jit(solution)/shard_map/tables/pallas_call | solution.py:285
  119.5 5.1 %all-to-all-done = bf16[96,2,4,256]{3,2,1,0:T(4,128)(2,1)S(1)} async-done(((bf16[96,2,4,256]{3,2,1,0:T(4,128)(2,1)}), bf16[96,2,4,256]{3,2,1,0:T(4,128)(2,1)S(1)}, u32[]{:S(2)}, u32[]{:S(2)}) %all-to-all-start) | async-done | bytes 393248 | tf_op jit(solution)/shard_map/all_to_all | solution.py:395
  124.6 0.2 copy.72
  124.8 0.8 reshape.100.u_ref
  125.6 6.1 %mixer.1 = bf16[6,128,256]{2,1,0:T(8,128)(2,1)} custom-call(bf16[6,128,256]{2,1,0:T(8,128)(2,1)} %reshape.100.u_ref, bf16[6,256,256]{2,1,0:T(8,128)(2,1)} %get-tuple-element.8.within, bf16[6,256,256]{2,1,0:T(8,128)(2,1)} %get-tuple-element.9.enter, bf16[6,256,256]{2,1,0:T(8,128)(2,1)} %get-tuple-element.10.leave, f32[6,54,128]{2,1,0:T(8,128)} %get-tuple-element.16.p_re, ...), custom_call_target="tpu_custom_call" | custom-call | tf_op jit(solution)/shard_map/mixer/pallas_call | solution.py:336
  131.7 1.1 reshape.108
  132.8 0.9 copy.85
  133.7 9.1 %all-to-all-start.1 = ((bf16[96,2,4,256]{3,2,1,0:T(4,128)(2,1)}), bf16[96,2,4,256]{3,2,1,0:T(4,128)(2,1)S(1)}, u32[]{:S(2)}, u32[]{:S(2)}) async-start(bf16[96,2,4,256]{3,2,1,0:T(4,128)(2,1)} %bitcast.21), calls=%async_computation.1 | async-start | bytes 786432 | tf_op jit(solution)/shard_map/all_to_all | solution.py:402
  142.9 12.3 %all-to-all-done.1 = bf16[96,2,4,256]{3,2,1,0:T(4,128)(2,1)S(1)} async-done(((bf16[96,2,4,256]{3,2,1,0:T(4,128)(2,1)}), bf16[96,2,4,256]{3,2,1,0:T(4,128)(2,1)S(1)}, u32[]{:S(2)}, u32[]{:S(2)}) %all-to-all-start.1) | async-done | bytes 393248 | tf_op jit(solution)/shard_map/all_to_all | solution.py:402
  155.1 1.2 copy.86
  156.3 3.1 %copy.87 = bf16[2,4,16,96,16]{4,3,2,1,0:T(8,128)(2,1)S(1)} copy(bf16[2,4,16,96,16]{3,4,2,1,0:T(8,128)(2,1)} %bitcast.93) | data formatting | bytes 786432 | tf_op jit(solution)/shard_map/transpose | solution.py:404
  159.4 5.6 %reshape.111 = bf16[2,64,1536]{2,1,0:T(8,128)(2,1)S(1)} reshape(bf16[2,4,16,96,16]{4,3,2,1,0:T(8,128)(2,1)S(1)} %copy.87) | data formatting | bytes 786432 | tf_op jit(solution)/shard_map/reshape | solution.py:404
  165.0 0.0 all-gather.2.cloned.1.call-done.shard
  165.0 1.8 slice.38
  166.9 4.9 %slice.40 = bf16[16,192,768]{2,1,0:T(8,128)(2,1)} slice(bf16[16,288,768]{2,1,0:T(8,128)(2,1)} %bitcast.82), slice={[0:16], [96:288], [0:768]} | slice | bytes 9437184 | tf_op jit(solution)/shard_map/slice | solution.py:380
  171.8 11.6 %swap.1 = bf16[1,4608,768]{2,1,0:T(8,128)(2,1)} custom-call(bf16[4608,768]{1,0:T(8,128)(2,1)} %all-gather.2.cloned.1.call-done.shard), custom_call_target="tpu_custom_call" | custom-call | tf_op jit(solution)/shard_map/swap/pallas_call | solution.py:229
  183.5 2.0 slice.39
  185.4 2.8 %slice.41 = bf16[16,192,768]{2,1,0:T(8,128)(2,1)S(1)} slice(bf16[16,288,768]{2,1,0:T(8,128)(2,1)} %bitcast.84), slice={[0:16], [96:288], [0:768]} | slice | bytes 9437184 | tf_op jit(solution)/shard_map/slice | solution.py:380
  188.3 0.9 fusion.21
  189.2 1.0 fusion.7
  190.1 1.6 fusion.18
  191.8 0.0 copy-start.4
  191.8 1.7 multiply_reduce_fusion
  193.5 1.1 multiply_convert_fusion
  (29 shorter events, 0.1 us)
Async XLA Ops:
  6.5 158.5 %all-gather.2.cloned.1.call-start = ((), (), s32[]{:S(2)}) async-start(), calls=%async_computation.2 | async-start | bytes 7520256 | tf_op jit(solution)/shard_map/all_gather | solution.py:374
  8.4 64.8 %copy-start = (bf16[2,64,3072]{2,1,0:T(8,128)(2,1)S(1)}, bf16[2,64,3072]{2,1,0:T(8,128)(2,1)}, u32[]{:S(2)}) copy-start(bf16[2,64,3072]{2,1,0:T(8,128)(2,1)} %param.12) | copy-start | bytes 2359300
  8.4 65.0 %copy-start.3 = (f32[3072]{0:T(1024)S(1)}, f32[3072]{0:T(1024)}, u32[]{:S(2)}) copy-start(f32[3072]{0:T(1024)} %param.13) | copy-start | bytes 36868
  83.0 22.8 %copy-start.1 = (f32[2,96,64]{1,2,0:T(8,128)S(1)}, f32[2,96,64]{1,2,0:T(8,128)}, u32[]{:S(2)}) copy-start(f32[2,96,64]{1,2,0:T(8,128)} %param.16) | copy-start | bytes 147460
  83.0 22.8 %copy-start.2 = (f32[2,96,64]{1,2,0:T(8,128)S(1)}, f32[2,96,64]{1,2,0:T(8,128)}, u32[]{:S(2)}) copy-start(f32[2,96,64]{1,2,0:T(8,128)} %param.15) | copy-start | bytes 147460
  85.6 22.0 %copy-start.6 = (f32[2,96]{1,0:T(2,128)S(1)}, f32[2,96]{1,0:T(2,128)}, u32[]{:S(2)}) copy-start(f32[2,96]{1,0:T(2,128)} %param.17) | copy-start | bytes 2308
  87.7 36.9 %all-to-all-start = ((bf16[96,2,4,256]{3,2,1,0:T(4,128)(2,1)}), bf16[96,2,4,256]{3,2,1,0:T(4,128)(2,1)S(1)}, u32[]{:S(2)}, u32[]{:S(2)}) async-start(bf16[96,2,4,256]{3,2,1,0:T(4,128)(2,1)} %copy.71), calls=%async_computation | async-start | bytes 786432 | tf_op jit(solution)/shard_map/all_to_all | solution.py:395
  107.9 4.5 %copy-start.5 = (f32[1536]{0:T(1024)S(1)}, f32[1536]{0:T(1024)}, u32[]{:S(2)}) copy-start(f32[1536]{0:T(1024)} %param.20) | copy-start | bytes 18436
  133.7 21.4 %all-to-all-start.1 = ((bf16[96,2,4,256]{3,2,1,0:T(4,128)(2,1)}), bf16[96,2,4,256]{3,2,1,0:T(4,128)(2,1)S(1)}, u32[]{:S(2)}, u32[]{:S(2)}) async-start(bf16[96,2,4,256]{3,2,1,0:T(4,128)(2,1)} %bitcast.21), calls=%async_computation.1 | async-start | bytes 786432 | tf_op jit(solution)/shard_map/all_to_all | solution.py:402
  183.5 6.7 %slice-start = ((s8[4718592]{0:T(1024)(128)(4,1)}), s8[4194304]{0:T(1024)(128)(4,1)S(1)}, s32[]{:S(2)}) async-start(s8[4718592]{0:T(1024)(128)(4,1)} %bitcast.86), calls=%async_computation.3 | async-start | bytes 8388608
  185.4 4.7 %slice-start.1 = ((s8[4718592]{0:T(1024)(128)(4,1)}), s8[524288]{0:T(1024)(128)(4,1)S(1)}, s32[]{:S(2)}) async-start(s8[4718592]{0:T(1024)(128)(4,1)} %bitcast.86), calls=%async_computation.4 | async-start | bytes 1048576
  191.8 1.8 copy-start.4
Sparse Core Ops, SparseCore 0:
  10.1 135.0 all-gather.1
